TPU v7x, 128 devices: a whole 4x4x4 slice. The times are simulated.
128 devices in a mesh: sp: 16 (over z, x), tp: 8 (over y, core).
Axes of the slice: x: 4, y: 4, z: 4, core: 2. Of those that a mesh axis runs over, the one named last changes fastest.
Arguments:
- latent: bfloat16 [32768, 2048], P(('sp', 'tp')), may hold values from -8 to 8
- context: bfloat16 [512, 2048], P('sp'), may hold values from -8 to 8
- latent_condition: bfloat16 [2048], replicated, may hold values from -4 to 4
- context_condition: bfloat16 [2048], replicated, may hold values from -4 to 4
- shift_weight: bfloat16 [2048, 2048], P('sp', 'tp'), may hold values from -0.125 to 0.125
- scale_weight: bfloat16 [2048, 2048], P('sp', 'tp'), may hold values from -0.125 to 0.125
- gate_weight: bfloat16 [2048, 2048], P('sp', 'tp'), may hold values from -0.125 to 0.125
- norm_gain: float32 [2048], replicated, may hold values from 0.1 to 1.9
- query_weight: bfloat16 [2048, 512], replicated, may hold values from -0.125 to 0.125
- key_weight: bfloat16 [2048, 512], replicated, may hold values from -0.125 to 0.125
- value_weight: bfloat16 [2048, 1024], replicated, may hold values from -0.125 to 0.125
- outgate_weight: bfloat16 [2048, 1024], replicated, may hold values from -0.125 to 0.125
- down_weight: bfloat16 [2048, 32], replicated, may hold values from -0.125 to 0.125
- up_weight: bfloat16 [32, 512], replicated, may hold values from -2 to 2
- decay_bias: float32 [512], replicated, as said below
- out_weight: bfloat16 [1024, 2048], replicated, may hold values from -0.1875 to 0.1875
- post_gain: float32 [2048], replicated, may hold values from 0.1 to 1.9
Outputs:
- updated: bfloat16 [32768, 2048], P(('sp', 'tp'))
Inputs may be any that keep to these rules, and one draw needn't show every extreme that they name: decay_bias is at least 0; counting heads from 0, the channels of heads 1, 3, 5, … are at least log(2048) + 2, those of heads 0, 2, 4, … at most 1.5.
All inputs are finite; a program needn't handle non-finite values.
Results may differ from a plain program's by a relative error of at most 0.0035.
The roundings to bfloat16 on the way count: a program that leaves them out, or rounds other values in their place, can miss the bound.
Values may be sent and summed in bfloat16 or wider, within the bound.
A program may use at most 192 MiB of HBM per device.

v0:
```python
import jax
import jax.numpy as jnp
from jax import lax
from jax.sharding import Mesh
from jax.sharding import PartitionSpec as P

HEADS = 16
DK = 32
DV = 64
BLOCK = 32
SP = ("sp_0", "sp_1")
TP = ("tp_0", "tp_1")
SP_TP = ("sp_0", "sp_1", "tp_0", "tp_1")


epsilon = 1e-06
decay_temper = 16.0
highest = lax.Precision.HIGHEST


def by_axis(x, axes):
    for axis in axes:
        x = lax.psum(x, axis)
    return x


def in_one_piece(arrays, axis, dim, along):
    ends, at = ([], 0)
    for a in arrays[:-1]:
        at += a.shape[along]
        ends.append(at)
    both = jnp.concatenate(arrays, axis=along)
    return tuple(jnp.split(lax.all_gather(both, axis, axis=dim, tiled=True), ends, axis=along))


def gather_axes(x, axes, dim):
    if not axes:
        return x
    nearer = lax.all_gather(x, axes[-1], axis=dim, tiled=True)
    return gather_axes(nearer, axes[:-1], dim)


def neutral_like(x, identity):
    return jax.tree.map(
        lambda part, zero: jnp.zeros_like(part) + jnp.asarray(zero, part.dtype), x, identity
    )


def carried_in(x, axes, combine, identity, reverse):
    before = start = neutral_like(x, identity)
    total = x
    for axis in reversed(axes):
        peers, mine = (lax.axis_size(axis), lax.axis_index(axis))
        pieces = jax.tree.map(lambda part: lax.all_gather(part, axis), total)
        inside, total = (start, start)
        for k in reversed(range(peers)) if reverse else range(peers):
            passed = k > mine if reverse else k < mine
            total = combine(total, jax.tree.map(lambda part: part[k], pieces))
            inside = jax.tree.map(lambda new, old: jnp.where(passed, new, old), total, inside)
        before = combine(inside, before)
    return before


def rms_factor(values):
    return lax.rsqrt(jnp.mean(values * values, axis=-1, keepdims=True) + epsilon)


def stored(values):
    return lax.optimization_barrier(values.astype(jnp.bfloat16))


def modulated(tokens, norm_gain, shift_row, scale_row):
    values = tokens.astype(jnp.float32)
    return (values * rms_factor(values) * norm_gain * (1.0 + scale_row) + shift_row).astype(
        jnp.bfloat16
    )


def project(normed, weight):
    return jnp.dot(normed, weight, preferred_element_type=jnp.float32)


def log_decays(normed, down_weight, up_weight, decay_bias):
    low_rank = project(normed, down_weight).astype(jnp.bfloat16)
    return jax.nn.log_sigmoid(project(low_rank, up_weight) + decay_bias) / decay_temper


def weighted_state(key_rows, value_rows, weights):
    row_count = key_rows.shape[0]
    scaled = (key_rows.astype(jnp.float32) * weights).reshape(row_count, HEADS, DK)
    value_heads = value_rows.astype(jnp.float32).reshape(row_count, HEADS, DV)
    return jnp.einsum("sha,she->hae", scaled, value_heads, precision=highest)


def segment_states(key_rows, value_rows, log_decay):
    inclusive = jnp.cumsum(log_decay, axis=0)
    total_log = inclusive[-1]
    after_log = total_log - inclusive
    before_log = inclusive - log_decay
    return (
        weighted_state(key_rows, value_rows, jnp.exp(after_log)),
        weighted_state(key_rows, value_rows, jnp.exp(before_log)),
        total_log,
    )


def context_projections(
    rows_in,
    norm_gain,
    shift_row,
    scale_row,
    key_weight,
    value_weight,
    down_weight,
    up_weight,
    decay_bias,
):
    ctx_normed = modulated(rows_in, norm_gain, shift_row, scale_row)
    ctx_keys = stored(project(ctx_normed, key_weight))
    ctx_values = stored(project(ctx_normed, value_weight))
    ctx_log = log_decays(ctx_normed, down_weight, up_weight, decay_bias)
    return segment_states(ctx_keys, ctx_values, ctx_log)


def block_terms(query_heads, key_heads, value_heads, log_heads):
    block_count = query_heads.shape[0] // BLOCK
    q_blocks = query_heads.reshape(block_count, BLOCK, HEADS, DK)
    k_blocks = key_heads.reshape(block_count, BLOCK, HEADS, DK)
    v_blocks = value_heads.reshape(block_count, BLOCK, HEADS, DV)
    inside = jnp.cumsum(log_heads.reshape(block_count, BLOCK, HEADS, DK), axis=1)
    closing = inside[:, -1]
    q_decayed = q_blocks * jnp.exp(inside)
    k_decayed = k_blocks * jnp.exp(-inside)
    scores = jnp.einsum("ntha,nsha->nhts", q_decayed, k_decayed, precision=highest)
    lower_mask = jnp.tril(jnp.ones((BLOCK, BLOCK), bool))
    scores = jnp.where(lower_mask, scores, 0.0)
    within = jnp.einsum("nhts,nshe->nthe", scores, v_blocks, precision=highest)
    summary = jnp.einsum(
        "nsha,nshe->nhae",
        k_blocks * jnp.exp(closing[:, None] - inside),
        v_blocks,
        precision=highest,
    )
    return (q_decayed, within, closing, summary)


def carried_states(closing, summary):
    block_count = closing.shape[0]
    opening = jnp.cumsum(closing, axis=0) - closing
    total_log = opening[-1] + closing[-1]
    boundaries = jnp.concatenate([opening, total_log[None]], axis=0)
    gap_logs = boundaries[:, None] - (opening + closing)[None]
    earlier = jnp.arange(block_count + 1)[:, None] > jnp.arange(block_count)[None, :]
    weights = jnp.exp(jnp.where(earlier[:, :, None, None], gap_logs, -jnp.inf))
    carried = jnp.einsum("nmha,mhae->nhae", weights, summary, precision=highest)
    return (opening, total_log, carried)


def block_output(terms, opening, carried, start_state):
    entering = carried[:-1] + jnp.exp(opening)[..., None] * start_state[None]
    across = jnp.einsum("ntha,nhae->nthe", terms[0], entering, precision=highest)
    return (terms[1] + across).reshape(-1, HEADS, DV)


def chain_combine(earlier_part, later_part):
    return (
        earlier_part[0] + later_part[0],
        jnp.exp(later_part[0])[..., None] * earlier_part[1] + later_part[1],
    )


def shards(
    latent,
    context,
    latent_condition,
    context_condition,
    shift_weight,
    scale_weight,
    gate_weight,
    norm_gain,
    query_weight,
    key_weight,
    value_weight,
    outgate_weight,
    down_weight,
    up_weight,
    decay_bias,
    out_weight,
    post_gain,
):
    conditions = jnp.stack([latent_condition, context_condition])
    cond_act = jax.nn.silu(conditions.astype(jnp.float32)).astype(jnp.bfloat16)
    row_share = shift_weight.shape[0]
    cond_rows = lax.dynamic_slice_in_dim(cond_act, lax.axis_index(SP) * row_share, row_share, 1)
    shift_part = project(cond_rows, shift_weight)
    scale_part = project(cond_rows, scale_weight)
    gate_part = project(cond_rows, gate_weight)
    shift_sum, scale_sum, gate_sum = (
        by_axis(shift_part, SP),
        by_axis(scale_part, SP),
        by_axis(gate_part, SP),
    )
    shifts, scales, gates = in_one_piece((shift_sum, scale_sum, gate_sum), TP, 1, 0)
    gathered = gather_axes(context, SP, 0)
    ctx_forward, ctx_backward, total_log = context_projections(
        gathered,
        norm_gain,
        shifts[1],
        scales[1],
        key_weight,
        value_weight,
        down_weight,
        up_weight,
        decay_bias,
    )
    normed = modulated(latent, norm_gain, shifts[0], scales[0])
    row_count = latent.shape[0]
    query_rows = stored(project(normed, query_weight))
    key_rows = stored(project(normed, key_weight))
    value_rows = stored(project(normed, value_weight))
    outgate_rows = stored(project(normed, outgate_weight))
    log_decay = log_decays(normed, down_weight, up_weight, decay_bias)
    query_heads = query_rows.astype(jnp.float32).reshape(row_count, HEADS, DK) * DK ** (-0.5)
    key_heads = key_rows.astype(jnp.float32).reshape(row_count, HEADS, DK)
    value_heads = value_rows.astype(jnp.float32).reshape(row_count, HEADS, DV)
    log_heads = log_decay.reshape(row_count, HEADS, DK)
    forward_terms = block_terms(query_heads, key_heads, value_heads, log_heads)
    backward_terms = block_terms(
        jnp.flip(query_heads, 0),
        jnp.flip(key_heads, 0),
        jnp.flip(value_heads, 0),
        jnp.flip(log_heads, 0),
    )
    forward_open, forward_total, forward_carried = carried_states(
        forward_terms[2], forward_terms[3]
    )
    backward_open, backward_total, backward_carried = carried_states(
        backward_terms[2], backward_terms[3]
    )
    zero_log = jnp.zeros((HEADS, DK), jnp.float32)
    zero_state = jnp.zeros((HEADS, DK, DV), jnp.float32)
    prior_log, prior_state = carried_in(
        (forward_total, forward_carried[-1]), SP_TP, chain_combine, (zero_log, zero_state), False
    )
    later_log, later_state = carried_in(
        (backward_total, backward_carried[-1]), SP_TP, chain_combine, (zero_log, zero_state), True
    )
    forward_start = prior_state + jnp.exp(prior_log)[..., None] * ctx_forward
    backward_start = later_state + jnp.exp(later_log)[..., None] * ctx_backward
    forward_out = block_output(forward_terms, forward_open, forward_carried, forward_start)
    backward_out = jnp.flip(
        block_output(backward_terms, backward_open, backward_carried, backward_start), 0
    )
    mixed_heads = forward_out + backward_out
    normalized = mixed_heads * rms_factor(mixed_heads)
    gate_heads = jax.nn.silu(outgate_rows.astype(jnp.float32).reshape(row_count, HEADS, DV))
    gated = (normalized * gate_heads).reshape(row_count, HEADS * DV).astype(jnp.bfloat16)
    branch = stored(project(gated, out_weight)).astype(jnp.float32)
    result = latent.astype(jnp.float32) + gates[0] * (branch * rms_factor(branch)) * post_gain
    return result.astype(jnp.bfloat16)


def solution(mesh):
    torus = Mesh(mesh.devices.reshape(4, 4, 4, 2), ("sp_0", "sp_1", "tp_0", "tp_1"))
    placed = (
        P(SP_TP, None),
        P(SP, None),
        P(),
        P(),
        P(SP, TP),
        P(SP, TP),
        P(SP, TP),
        P(),
        P(),
        P(),
        P(),
        P(),
        P(),
        P(),
        P(),
        P(),
        P(),
    )
    return jax.shard_map(
        shards, mesh=torus, in_specs=placed, out_specs=P(SP_TP, None), check_vma=False
    )
```

profile of v0, /device:TPU:0, one launch (start us, length us, event | category | flops | bytes accessed | tf_op | source)
XLA Modules:
  0.0 441.8 jit_solution(8463039733386729428)
XLA Ops:
  6.6 15.1 %all_gather.80 = bf16[128,2048]{1,0:T(8,128)(2,1)} all-gather(bf16[32,2048]{1,0:T(8,128)(2,1)} %param.18), channel_id=1, replica_groups=mesh['sp_0'=4,'sp_1'=4,'tp_0'=4,'tp_1'=2] {'sp_1'}, dimensions={0}, use_global_device_ids=true | all-gather | bytes 655360 | tf_op jit(solution)/shard_map/all_gather | solution.py:39
  26.0 11.9 %all-reduce.1 = (f32[2,256]{1,0:T(2,128)S(1)}, f32[2,256]{1,0:T(2,128)S(1)}, f32[2,256]{1,0:T(2,128)S(1)}) all-reduce(f32[2,256]{1,0:T(2,128)S(1)} %fusion.121, f32[2,256]{1,0:T(2,128)S(1)} %fusion.117, f32[2,256]{1,0:T(2,128)S(1)} %fusion.119), channel_id=1, replica_groups=mesh['sp_0'=4,'sp_1'=4,'tp_0'=4,'tp_1'=2] {'sp_0'}, use_global_device_ids=true, to_apply=%region_4.5 | all-reduce | flops 1536 | bytes 12288 | tf_op jit(solution)/shard_map/psum | solution.py:23
  38.0 9.4 %all-reduce = (f32[2,256]{1,0:T(2,128)S(1)}, f32[2,256]{1,0:T(2,128)S(1)}, f32[2,256]{1,0:T(2,128)S(1)}) all-reduce(f32[2,256]{1,0:T(2,128)S(1)} %get-tuple-element.8, f32[2,256]{1,0:T(2,128)S(1)} %get-tuple-element.9, f32[2,256]{1,0:T(2,128)S(1)} %get-tuple-element.10), channel_id=1, replica_groups=mesh['sp_0'=4,'sp_1'=4,'tp_0'=4,'tp_1'=2] {'sp_1'}, use_global_device_ids=true, to_apply=%region_5.6 | all-reduce | flops 1536 | bytes 12288 | tf_op jit(solution)/shard_map/psum | solution.py:23
  47.4 13.3 %all_gather.71 = f32[6,2048]{1,0:T(8,128)S(1)} all-gather(f32[6,256]{1,0:T(8,128)S(1)} %pad_maximum_fusion.2), channel_id=1, replica_groups=mesh['sp_0'=4,'sp_1'=4,'tp_0'=4,'tp_1'=2] {'tp_0','tp_1'}, dimensions={1}, use_global_device_ids=true | all-gather | bytes 55296 | tf_op jit(solution)/shard_map/all_gather | solution.py:33
  61.7 1.9 fusion.79
  63.6 2.8 reshape_reshape.10
  70.2 1.9 all_gather.72
  73.5 1.8 reshape_reshape.11
  76.2 2.0 copy.139
  78.3 2.3 convolution_convert_fusion.6
  82.4 4.3 convolution_convert_fusion.4
  86.7 1.8 reshape_reshape.9
  88.5 2.2 copy.135
  90.7 1.9 rev.19
  92.7 3.5 copy.161
  96.1 1.8 fusion.138
  99.3 2.0 all_gather.82
  101.3 4.6 %convolution_convert_fusion.3 = bf16[256,1024]{1,0:T(8,128)(2,1)} fusion(bf16[2048,1024]{1,0:T(8,128)(2,1)} %param.28, bf16[256,2048]{1,0:T(8,128)(2,1)} %param.17, f32[2048]{0:T(1024)S(1)} %bitcast.380, f32[2048]{0:T(1024)S(1)} %bitcast.385, f32[2048]{0:T(1024)S(1)} %copy-done.103, f32[256]{0:T(256)S(1)} %copy-done.98), kind=kOutput, calls=%fused_computation.73 | convolution fusion | flops 1077149696 | bytes 5792768 | tf_op jit(solution)/shard_map/dot_general | solution.py:80
  105.9 2.2 copy.160
  108.2 13.2 %mul.594 = f32[8,32,16,32]{3,2,1,0:T(8,128)} reshape(f32[256,512]{1,0:T(8,128)} %broadcast_multiply_fusion.1) | data formatting | bytes 1048576 | tf_op jit(solution)/shard_map/mul | solution.py:223
  122.4 1.8 copy.122
  124.2 5.6 %exponential_multiply_fusion.4 = (f32[8,32,16,32]{3,2,1,0:T(8,128)}, f32[8,32,16,32]{3,2,1,0:T(8,128)S(1)}, f32[8,32,16,32]{3,2,1,0:T(8,128)}) fusion(f32[8,32,16,32]{3,2,1,0:T(8,128)} %reshape_reshape.11, f32[8,32,16,32]{3,2,1,0:T(8,128)} %copy-done.13, f32[8,16,32]{2,1,0:T(8,128)S(1)} %slice_bitcast_fusion.9, f32[8,32,16,32]{3,2,1,0:T(8,128)} %mul.594), kind=kLoop, calls=%fused_computation.58 | loop fusion | flops 655360 | bytes 3162112 | tf_op jit(solution)/shard_map/mul | solution.py:133
  129.8 2.3 fusion.24
  132.1 8.4 %convolution_bitcast_fusion.1 = f32[9,16,32,64]{3,0,2,1:T(8,128)S(1)} fusion(f32[8,16,32,64]{3,2,1,0:T(8,128)S(1)} %fusion.24, f32[8,16,32]{0,2,1:T(8,128)S(1)} %copy.123, f32[9,16,32]{0,2,1:T(8,128)S(1)} %copy-done.35, pred[9,8]{0,1:T(8,128)(4,1)S(1)} %copy-done.95), kind=kOutput, calls=%fused_computation.16 | convolution fusion | flops 28385280 | bytes 2263112 | tf_op jit(solution)/shard_map/nmha,mhae->nhae/dot_general | solution.py:155
  140.7 2.2 all_gather.76
  143.9 15.3 %all_gather.77 = f32[4,16,32,64]{3,2,1,0:T(8,128)S(1)} all-gather(f32[1,16,32,64]{3,2,1,0:T(8,128)S(1)} %multiply_add_fusion.5), channel_id=1, replica_groups=mesh['sp_0'=4,'sp_1'=4,'tp_0'=4,'tp_1'=2] {'tp_0'}, dimensions={0}, use_global_device_ids=true | all-gather | bytes 655360 | tf_op jit(solution)/shard_map/all_gather | solution.py:54
  159.2 11.9 %all_gather.73 = f32[4,16,32]{2,1,0:T(8,128)S(1)} all-gather(f32[1,16,32]{2,1,0:T(8,128)S(1)} %get-tuple-element.22), channel_id=1, replica_groups=mesh['sp_0'=4,'sp_1'=4,'tp_0'=4,'tp_1'=2] {'tp_0'}, dimensions={0}, use_global_device_ids=true | all-gather | bytes 10240 | tf_op jit(solution)/shard_map/all_gather | solution.py:54
  171.5 15.2 %all_gather.78 = f32[4,16,32,64]{3,2,1,0:T(8,128)S(1)} all-gather(f32[1,16,32,64]{3,2,1,0:T(8,128)S(1)} %multiply_add_fusion.4), channel_id=1, replica_groups=mesh['sp_0'=4,'sp_1'=4,'tp_0'=4,'tp_1'=2] {'sp_1'}, dimensions={0}, use_global_device_ids=true | all-gather | bytes 655360 | tf_op jit(solution)/shard_map/all_gather | solution.py:54
  186.8 11.9 %all_gather.74 = f32[4,16,32]{2,1,0:T(8,128)S(1)} all-gather(f32[1,16,32]{2,1,0:T(8,128)S(1)} %get-tuple-element.65), channel_id=1, replica_groups=mesh['sp_0'=4,'sp_1'=4,'tp_0'=4,'tp_1'=2] {'sp_1'}, dimensions={0}, use_global_device_ids=true | all-gather | bytes 10240 | tf_op jit(solution)/shard_map/all_gather | solution.py:54
  199.1 14.6 %all_gather.79 = f32[4,16,32,64]{3,2,1,0:T(8,128)} all-gather(f32[1,16,32,64]{3,2,1,0:T(8,128)S(1)} %multiply_add_fusion.3), channel_id=1, replica_groups=mesh['sp_0'=4,'sp_1'=4,'tp_0'=4,'tp_1'=2] {'sp_0'}, dimensions={0}, use_global_device_ids=true | all-gather | bytes 655360 | tf_op jit(solution)/shard_map/all_gather | solution.py:54
  213.7 12.6 %all_gather.75 = f32[4,16,32]{2,1,0:T(8,128)} all-gather(f32[1,16,32]{2,1,0:T(8,128)S(1)} %get-tuple-element.60), channel_id=1, replica_groups=mesh['sp_0'=4,'sp_1'=4,'tp_0'=4,'tp_1'=2] {'sp_0'}, dimensions={0}, use_global_device_ids=true | all-gather | bytes 10240 | tf_op jit(solution)/shard_map/all_gather | solution.py:54
  227.4 1.9 rev.20
  229.3 3.6 copy.142
  232.9 2.0 reverse.3
  234.8 1.9 broadcast_multiply_fusion
  236.7 3.5 copy.138
  240.3 2.6 rev.17
  242.9 3.8 copy.136
  249.3 5.8 %exponential_multiply_fusion.1 = (f32[8,32,16,32]{3,2,1,0:T(8,128)}, f32[8,32,16,32]{3,2,1,0:T(8,128)S(1)}, f32[8,32,16,32]{3,2,1,0:T(8,128)}) fusion(f32[8,32,16,32]{3,2,1,0:T(8,128)} %bitcast.348, f32[8,32,16,32]{3,2,1,0:T(8,128)} %copy-done.12, f32[8,16,32]{2,1,0:T(8,128)} %slice_bitcast_fusion.8, f32[8,32,16,32]{3,2,1,0:T(8,128)} %bitcast.349), kind=kLoop, calls=%fused_computation.49 | loop fusion | flops 655360 | bytes 3162112 | tf_op jit(solution)/shard_map/mul | solution.py:133
  255.1 4.5 %fusion.17 = f32[8,16,32,64]{3,2,1,0:T(8,128)S(1)} fusion(f32[8,32,16,32]{3,2,1,0:T(8,128)S(1)} %get-tuple-element.24, f32[8,32,16,64]{3,2,1,0:T(8,128)S(1)} %bitcast.345), kind=kOutput, calls=%fused_computation.31 | convolution fusion | flops 100663296 | bytes 2621440 | tf_op jit(solution)/shard_map/nsha,nshe->nhae/dot_general | solution.py:138
  259.6 8.6 %convolution_bitcast_fusion = f32[9,16,32,64]{3,0,2,1:T(8,128)S(1)} fusion(f32[8,16,32,64]{3,2,1,0:T(8,128)S(1)} %fusion.17, f32[8,16,32]{0,2,1:T(8,128)S(1)} %copy-done.33, f32[9,16,32]{0,2,1:T(8,128)S(1)} %copy-done.34, pred[9,8]{0,1:T(8,128)(4,1)S(1)} %copy-done.96), kind=kOutput, calls=%fused_computation.15 | convolution fusion | flops 28385280 | bytes 2263112 | tf_op jit(solution)/shard_map/nmha,mhae->nhae/dot_general | solution.py:155
  268.2 2.0 copy-done.10
  270.4 2.3 all_gather.86
  273.4 11.9 %all_gather.83 = f32[4,16,32]{2,1,0:T(8,128)S(1)} all-gather(f32[1,16,32]{2,1,0:T(8,128)S(1)} %get-tuple-element.17), channel_id=1, replica_groups=mesh['sp_0'=4,'sp_1'=4,'tp_0'=4,'tp_1'=2] {'tp_0'}, dimensions={0}, use_global_device_ids=true | all-gather | bytes 10240 | tf_op jit(solution)/shard_map/all_gather | solution.py:54
  285.9 11.9 %all_gather.84 = f32[4,16,32]{2,1,0:T(8,128)S(1)} all-gather(f32[1,16,32]{2,1,0:T(8,128)S(1)} %get-tuple-element.50), channel_id=1, replica_groups=mesh['sp_0'=4,'sp_1'=4,'tp_0'=4,'tp_1'=2] {'sp_1'}, dimensions={0}, use_global_device_ids=true | all-gather | bytes 10240 | tf_op jit(solution)/shard_map/all_gather | solution.py:54
  298.4 12.6 %all_gather.85 = f32[4,16,32]{2,1,0:T(8,128)} all-gather(f32[1,16,32]{2,1,0:T(8,128)S(1)} %get-tuple-element.45), channel_id=1, replica_groups=mesh['sp_0'=4,'sp_1'=4,'tp_0'=4,'tp_1'=2] {'sp_0'}, dimensions={0}, use_global_device_ids=true | all-gather | bytes 10240 | tf_op jit(solution)/shard_map/all_gather | solution.py:54
  314.1 14.0 %all_gather.87 = f32[4,16,32,64]{3,2,1,0:T(8,128)S(1)} all-gather(f32[1,16,32,64]{3,2,1,0:T(8,128)S(1)} %multiply_add_fusion.2), channel_id=1, replica_groups=mesh['sp_0'=4,'sp_1'=4,'tp_0'=4,'tp_1'=2] {'tp_0'}, dimensions={0}, use_global_device_ids=true | all-gather | bytes 655360 | tf_op jit(solution)/shard_map/all_gather | solution.py:54
  328.5 14.0 %all_gather.88 = f32[4,16,32,64]{3,2,1,0:T(8,128)S(1)} all-gather(f32[1,16,32,64]{3,2,1,0:T(8,128)S(1)} %multiply_add_fusion.1), channel_id=1, replica_groups=mesh['sp_0'=4,'sp_1'=4,'tp_0'=4,'tp_1'=2] {'sp_1'}, dimensions={0}, use_global_device_ids=true | all-gather | bytes 655360 | tf_op jit(solution)/shard_map/all_gather | solution.py:54
  342.8 14.6 %all_gather.89 = f32[4,16,32,64]{3,2,1,0:T(8,128)} all-gather(f32[1,16,32,64]{3,2,1,0:T(8,128)S(1)} %multiply_add_fusion), channel_id=1, replica_groups=mesh['sp_0'=4,'sp_1'=4,'tp_0'=4,'tp_1'=2] {'sp_0'}, dimensions={0}, use_global_device_ids=true | all-gather | bytes 655360 | tf_op jit(solution)/shard_map/all_gather | solution.py:54
  358.2 6.0 %fusion.26 = f32[8,16,32,32]{3,2,1,0:T(8,128)} fusion(f32[8,32,16,32]{3,2,1,0:T(8,128)S(1)} %copy-done.15, f32[8,32,16,32]{3,2,1,0:T(8,128)S(1)} %copy-done.2), kind=kOutput, calls=%fused_computation.40 | convolution fusion | flops 50331648 | bytes 1572864 | tf_op jit(solution)/shard_map/ntha,nsha->nhts/dot_general | solution.py:134
  364.2 6.0 %fusion.19 = f32[8,16,32,32]{3,2,1,0:T(8,128)} fusion(f32[8,32,16,32]{3,2,1,0:T(8,128)S(1)} %copy-done.17, f32[8,32,16,32]{3,2,1,0:T(8,128)S(1)} %copy-done.4), kind=kOutput, calls=%fused_computation.33 | convolution fusion | flops 50331648 | bytes 1572864 | tf_op jit(solution)/shard_map/ntha,nsha->nhts/dot_general | solution.py:134
  370.2 2.2 fusion
  372.5 2.1 convolution_convert_fusion.2
  374.6 3.1 fusion.50
  384.2 1.9 convert_multiply_fusion.6
  387.4 6.2 %convolution_convert_fusion.1 = bf16[512,1024]{1,0:T(8,128)(2,1)} fusion(bf16[2048,1024]{1,0:T(8,128)(2,1)} %param.27, bf16[512,2048]{1,0:T(8,128)(2,1)} %all-gather.2.cloned.1.call-done, f32[2048]{0:T(1024)S(1)} %bitcast.372, f32[2048]{0:T(1024)S(1)} %bitcast.375, f32[2048]{0:T(1024)S(1)} %copy-done.104, f32[512]{0:T(512)S(1)} %add_rsqrt_fusion.1), kind=kOutput, calls=%fused_computation.67 | convolution fusion | flops 2154299392 | bytes 7366656 | tf_op jit(solution)/shard_map/dot_general | solution.py:80
  396.4 3.5 fusion.53
  401.5 3.1 fusion.21
  406.1 2.5 copy.134
  408.7 2.6 copy.159
  412.8 4.2 fusion.52
  418.6 3.0 fusion.14
  421.7 2.8 add_bitcast_fusion
  425.7 2.0 copy.158
  (294 shorter events, 52.2 us)
Async XLA Ops:
  6.5 66.2 %copy-start = (bf16[2048,512]{1,0:T(8,128)(2,1)S(1)}, bf16[2048,512]{1,0:T(8,128)(2,1)}, u32[]{:S(2)}) copy-start(bf16[2048,512]{1,0:T(8,128)(2,1)} %param.26) | copy-start | bytes 6291460
  6.5 54.8 %copy-start.22 = (bf16[256,2048]{1,0:T(8,128)(2,1)S(1)}, bf16[256,2048]{1,0:T(8,128)(2,1)}, u32[]{:S(2)}) copy-start(bf16[256,2048]{1,0:T(8,128)(2,1)} %param.17) | copy-start | bytes 3145732
  6.5 55.1 %copy-start.102 = (f32[2048]{0:T(1024)S(1)}, f32[2048]{0:T(1024)}, u32[]{:S(2)}) copy-start(f32[2048]{0:T(1024)} %param.24) | copy-start | bytes 24580
  6.5 55.1 %copy-start.101 = (bf16[32,512]{1,0:T(8,128)(2,1)S(1)}, bf16[32,512]{1,0:T(8,128)(2,1)}, u32[]{:S(2)}) copy-start(bf16[32,512]{1,0:T(8,128)(2,1)} %param.30) | copy-start | bytes 98308
  6.5 55.1 %copy-start.100 = (bf16[2048,32]{0,1:T(8,128)(2,1)S(1)}, bf16[2048,32]{0,1:T(8,128)(2,1)}, u32[]{:S(2)}) copy-start(bf16[2048,32]{0,1:T(8,128)(2,1)} %param.29) | copy-start | bytes 393220
  6.6 55.1 %copy-start.105 = (f32[512]{0:T(512)S(1)}, f32[512]{0:T(512)}, u32[]{:S(2)}) copy-start(f32[512]{0:T(512)} %param.31) | copy-start | bytes 6148
  6.6 363.6 %all-gather.2.cloned.1.call-start = ((), (), s32[]{:S(2)}) async-start(), calls=%async_computation | async-start | bytes 2621440 | tf_op jit(solution)/shard_map/all_gather | solution.py:39
  61.3 21.1 %copy-start.93 = (f32[1,2048]{1,0:T(1,128)}, f32[1,2048]{1,0:T(1,128)S(1)}, u32[]{:S(2)}) copy-start(f32[1,2048]{1,0:T(1,128)S(1)} %get-tuple-element.35) | copy-start | bytes 24580
  61.6 20.8 %copy-start.97 = (f32[256]{0:T(256)}, f32[256]{0:T(256)S(1)}, u32[]{:S(2)}) copy-start(f32[256]{0:T(256)S(1)} %add_rsqrt_fusion.3) | copy-start | bytes 3076
  96.1 5.2 %copy-start.94 = (f32[1,2048]{1,0:T(1,128)S(1)}, f32[1,2048]{1,0:T(1,128)}, u32[]{:S(2)}) copy-start(f32[1,2048]{1,0:T(1,128)} %copy-done.93) | copy-start | bytes 24580
  96.1 5.2 %copy-start.98 = (f32[256]{0:T(256)S(1)}, f32[256]{0:T(256)}, u32[]{:S(2)}) copy-start(f32[256]{0:T(256)} %copy-done.97) | copy-start | bytes 3076
  96.1 5.2 %copy-start.103 = (f32[2048]{0:T(1024)S(1)}, f32[2048]{0:T(1024)}, u32[]{:S(2)}) copy-start(f32[2048]{0:T(1024)} %param.24) | copy-start | bytes 24580
  132.1 10.8 %copy-start.40 = (f32[2,16,32]{2,1,0:T(8,128)S(1)}, f32[2,16,32]{2,1,0:T(8,128)}, u32[]{:S(2)}) copy-start(f32[2,16,32]{2,1,0:T(8,128)} %all_gather.72) | copy-start | bytes 12292
  140.5 31.0 %copy-start.8 = (f32[9,16,32,64]{3,0,2,1:T(8,128)}, f32[9,16,32,64]{3,0,2,1:T(8,128)S(1)}, u32[]{:S(2)}) copy-start(f32[9,16,32,64]{3,0,2,1:T(8,128)S(1)} %convolution_bitcast_fusion.1) | copy-start | bytes 3538948
  143.6 15.6 %copy-start.49 = (f32[16,32]{1,0:T(8,128)}, f32[16,32]{1,0:T(8,128)S(1)}, u32[]{:S(2)}) copy-start(f32[16,32]{1,0:T(8,128)S(1)} %get-tuple-element.72) | copy-start | bytes 6148
  143.6 15.6 %copy-start.51 = (f32[16,32]{1,0:T(8,128)}, f32[16,32]{1,0:T(8,128)S(1)}, u32[]{:S(2)}) copy-start(f32[16,32]{1,0:T(8,128)S(1)} %get-tuple-element.73) | copy-start | bytes 6148
  143.6 43.2 %copy-start.43 = (f32[1,16,32]{2,1,0:T(8,128)}, f32[1,16,32]{2,1,0:T(8,128)S(1)}, u32[]{:S(2)}) copy-start(f32[1,16,32]{2,1,0:T(8,128)S(1)} %get-tuple-element.22) | copy-start | bytes 6148
  159.2 39.9 %copy-start.18 = (f32[4,16,32,64]{3,2,1,0:T(8,128)}, f32[4,16,32,64]{3,2,1,0:T(8,128)S(1)}, u32[]{:S(2)}) copy-start(f32[4,16,32,64]{3,2,1,0:T(8,128)S(1)} %all_gather.77) | copy-start | bytes 1572868
  171.1 15.6 %copy-start.53 = (f32[16,32]{1,0:T(8,128)}, f32[16,32]{1,0:T(8,128)S(1)}, u32[]{:S(2)}) copy-start(f32[16,32]{1,0:T(8,128)S(1)} %get-tuple-element.66) | copy-start | bytes 6148
  171.1 15.6 %copy-start.55 = (f32[16,32]{1,0:T(8,128)}, f32[16,32]{1,0:T(8,128)S(1)}, u32[]{:S(2)}) copy-start(f32[16,32]{1,0:T(8,128)S(1)} %get-tuple-element.67) | copy-start | bytes 6148
  171.1 15.6 %copy-start.57 = (f32[16,32]{1,0:T(8,128)}, f32[16,32]{1,0:T(8,128)S(1)}, u32[]{:S(2)}) copy-start(f32[16,32]{1,0:T(8,128)S(1)} %get-tuple-element.68) | copy-start | bytes 6148
  171.1 42.6 %copy-start.59 = (f32[16,32]{1,0:T(8,128)}, f32[16,32]{1,0:T(8,128)S(1)}, u32[]{:S(2)}) copy-start(f32[16,32]{1,0:T(8,128)S(1)} %get-tuple-element.69) | copy-start | bytes 6148
  186.7 27.0 %copy-start.19 = (f32[4,16,32,64]{3,2,1,0:T(8,128)}, f32[4,16,32,64]{3,2,1,0:T(8,128)S(1)}, u32[]{:S(2)}) copy-start(f32[4,16,32,64]{3,2,1,0:T(8,128)S(1)} %all_gather.78) | copy-start | bytes 1572868
  198.7 27.7 %copy-start.61 = (f32[16,32]{1,0:T(8,128)}, f32[16,32]{1,0:T(8,128)S(1)}, u32[]{:S(2)}) copy-start(f32[16,32]{1,0:T(8,128)S(1)} %get-tuple-element.61) | copy-start | bytes 6148
  198.7 27.7 %copy-start.63 = (f32[16,32]{1,0:T(8,128)}, f32[16,32]{1,0:T(8,128)S(1)}, u32[]{:S(2)}) copy-start(f32[16,32]{1,0:T(8,128)S(1)} %get-tuple-element.62) | copy-start | bytes 6148
  198.7 27.6 %copy-start.65 = (f32[16,32]{1,0:T(8,128)}, f32[16,32]{1,0:T(8,128)S(1)}, u32[]{:S(2)}) copy-start(f32[16,32]{1,0:T(8,128)S(1)} %get-tuple-element.63) | copy-start | bytes 6148
  198.7 27.6 %copy-start.67 = (f32[16,32]{1,0:T(8,128)}, f32[16,32]{1,0:T(8,128)S(1)}, u32[]{:S(2)}) copy-start(f32[16,32]{1,0:T(8,128)S(1)} %get-tuple-element.64) | copy-start | bytes 6148
  249.3 5.8 %copy-start.6 = (f32[256,16,64]{2,1,0:T(8,128)S(1)}, f32[256,16,64]{2,1,0:T(8,128)}, u32[]{:S(2)}) copy-start(f32[256,16,64]{2,1,0:T(8,128)} %copy.136) | copy-start | bytes 3145732
  255.1 4.5 %copy-start.33 = (f32[8,16,32]{0,2,1:T(8,128)S(1)}, f32[8,16,32]{0,2,1:T(8,128)}, u32[]{:S(2)}) copy-start(f32[8,16,32]{0,2,1:T(8,128)} %copy.150) | copy-start | bytes 49156
  255.1 4.5 %copy-start.34 = (f32[9,16,32]{0,2,1:T(8,128)S(1)}, f32[9,16,32]{0,2,1:T(8,128)}, u32[]{:S(2)}) copy-start(f32[9,16,32]{0,2,1:T(8,128)} %copy.149) | copy-start | bytes 55300
  255.1 4.5 %copy-start.96 = (pred[9,8]{0,1:T(8,128)(4,1)S(1)}, pred[9,8]{0,1:T(8,128)(4,1)}, u32[]{:S(2)}) copy-start(pred[9,8]{0,1:T(8,128)(4,1)} %iota_compare_fusion.1) | copy-start | bytes 220
  259.6 13.1 %copy-start.42 = (f32[2,16,32]{2,1,0:T(8,128)S(1)}, f32[2,16,32]{2,1,0:T(8,128)}, u32[]{:S(2)}) copy-start(f32[2,16,32]{2,1,0:T(8,128)} %all_gather.82) | copy-start | bytes 12292
  273.4 12.5 %copy-start.45 = (f32[1,16,32]{2,1,0:T(8,128)}, f32[1,16,32]{2,1,0:T(8,128)S(1)}, u32[]{:S(2)}) copy-start(f32[1,16,32]{2,1,0:T(8,128)S(1)} %get-tuple-element.17) | copy-start | bytes 6148
  312.7 15.3 %copy-start.71 = (f32[16,32]{1,0:T(8,128)S(1)}, f32[16,32]{1,0:T(8,128)}, u32[]{:S(2)}) copy-start(f32[16,32]{1,0:T(8,128)} %get-tuple-element.51) | copy-start | bytes 6148
  312.7 15.3 %copy-start.73 = (f32[16,32]{1,0:T(8,128)S(1)}, f32[16,32]{1,0:T(8,128)}, u32[]{:S(2)}) copy-start(f32[16,32]{1,0:T(8,128)} %get-tuple-element.52) | copy-start | bytes 6148
  312.7 15.3 %copy-start.75 = (f32[16,32]{1,0:T(8,128)S(1)}, f32[16,32]{1,0:T(8,128)}, u32[]{:S(2)}) copy-start(f32[16,32]{1,0:T(8,128)} %get-tuple-element.53) | copy-start | bytes 6148
  312.7 15.3 %copy-start.77 = (f32[16,32]{1,0:T(8,128)S(1)}, f32[16,32]{1,0:T(8,128)}, u32[]{:S(2)}) copy-start(f32[16,32]{1,0:T(8,128)} %get-tuple-element.54) | copy-start | bytes 6148
  314.0 28.4 %copy-start.79 = (f32[16,32]{1,0:T(8,128)S(1)}, f32[16,32]{1,0:T(8,128)}, u32[]{:S(2)}) copy-start(f32[16,32]{1,0:T(8,128)} %get-tuple-element.46) | copy-start | bytes 6148
  314.0 28.4 %copy-start.81 = (f32[16,32]{1,0:T(8,128)S(1)}, f32[16,32]{1,0:T(8,128)}, u32[]{:S(2)}) copy-start(f32[16,32]{1,0:T(8,128)} %get-tuple-element.47) | copy-start | bytes 6148
  314.1 28.4 %copy-start.83 = (f32[16,32]{1,0:T(8,128)S(1)}, f32[16,32]{1,0:T(8,128)}, u32[]{:S(2)}) copy-start(f32[16,32]{1,0:T(8,128)} %get-tuple-element.48) | copy-start | bytes 6148
  314.1 28.4 %copy-start.85 = (f32[16,32]{1,0:T(8,128)S(1)}, f32[16,32]{1,0:T(8,128)}, u32[]{:S(2)}) copy-start(f32[16,32]{1,0:T(8,128)} %get-tuple-element.49) | copy-start | bytes 6148
  328.1 29.4 %copy-start.20 = (f32[4,16,32,64]{3,2,1,0:T(8,128)}, f32[4,16,32,64]{3,2,1,0:T(8,128)S(1)}, u32[]{:S(2)}) copy-start(f32[4,16,32,64]{3,2,1,0:T(8,128)S(1)} %all_gather.87) | copy-start | bytes 1572868
  328.1 29.3 %copy-start.41 = (f32[2,16,32]{2,1,0:T(8,128)S(1)}, f32[2,16,32]{2,1,0:T(8,128)}, u32[]{:S(2)}) copy-start(f32[2,16,32]{2,1,0:T(8,128)} %all_gather.72) | copy-start | bytes 12292
  328.1 29.3 %copy-start.44 = (f32[1,16,32]{2,1,0:T(8,128)S(1)}, f32[1,16,32]{2,1,0:T(8,128)}, u32[]{:S(2)}) copy-start(f32[1,16,32]{2,1,0:T(8,128)} %copy-done.43) | copy-start | bytes 6148
  328.1 30.0 %copy-start.46 = (f32[1,16,32]{2,1,0:T(8,128)S(1)}, f32[1,16,32]{2,1,0:T(8,128)}, u32[]{:S(2)}) copy-start(f32[1,16,32]{2,1,0:T(8,128)} %copy-done.45) | copy-start | bytes 6148
  328.5 29.6 %copy-start.38 = (f32[4,16,32]{2,1,0:T(8,128)S(1)}, f32[4,16,32]{2,1,0:T(8,128)}, u32[]{:S(2)}) copy-start(f32[4,16,32]{2,1,0:T(8,128)} %all_gather.75) | copy-start | bytes 24580
  328.5 29.7 %copy-start.39 = (f32[4,16,32]{2,1,0:T(8,128)S(1)}, f32[4,16,32]{2,1,0:T(8,128)}, u32[]{:S(2)}) copy-start(f32[4,16,32]{2,1,0:T(8,128)} %all_gather.85) | copy-start | bytes 24580
  328.5 29.7 %copy-start.2 = (f32[8,32,16,32]{3,2,1,0:T(8,128)S(1)}, f32[8,32,16,32]{3,2,1,0:T(8,128)}, u32[]{:S(2)}) copy-start(f32[8,32,16,32]{3,2,1,0:T(8,128)} %get-tuple-element.28) | copy-start | bytes 1572868
  328.5 29.7 %copy-start.15 = (f32[8,32,16,32]{3,2,1,0:T(8,128)S(1)}, f32[8,32,16,32]{3,2,1,0:T(8,128)}, u32[]{:S(2)}) copy-start(f32[8,32,16,32]{3,2,1,0:T(8,128)} %get-tuple-element.25) | copy-start | bytes 1572868
  342.5 15.7 %copy-start.21 = (f32[4,16,32,64]{3,2,1,0:T(8,128)}, f32[4,16,32,64]{3,2,1,0:T(8,128)S(1)}, u32[]{:S(2)}) copy-start(f32[4,16,32,64]{3,2,1,0:T(8,128)S(1)} %all_gather.88) | copy-start | bytes 1572868
  358.2 6.0 %copy-start.4 = (f32[8,32,16,32]{3,2,1,0:T(8,128)S(1)}, f32[8,32,16,32]{3,2,1,0:T(8,128)}, u32[]{:S(2)}) copy-start(f32[8,32,16,32]{3,2,1,0:T(8,128)} %get-tuple-element.27) | copy-start | bytes 1572868
  358.2 6.0 %copy-start.17 = (f32[8,32,16,32]{3,2,1,0:T(8,128)S(1)}, f32[8,32,16,32]{3,2,1,0:T(8,128)}, u32[]{:S(2)}) copy-start(f32[8,32,16,32]{3,2,1,0:T(8,128)} %get-tuple-element.23) | copy-start | bytes 1572868
  364.2 8.2 %copy-start.89 = (f32[1,2048]{1,0:T(1,128)S(1)}, f32[1,2048]{1,0:T(1,128)}, u32[]{:S(2)}) copy-start(f32[1,2048]{1,0:T(1,128)} %get-tuple-element.33) | copy-start | bytes 24580
  364.2 8.3 %copy-start.104 = (f32[2048]{0:T(1024)S(1)}, f32[2048]{0:T(1024)}, u32[]{:S(2)}) copy-start(f32[2048]{0:T(1024)} %param.24) | copy-start | bytes 24580
  408.6 4.1 copy-start.31
  408.6 4.1 copy-start.69
  408.6 4.1 copy-start.70
  408.6 4.1 copy-start.72
  408.6 4.1 copy-start.74
  408.6 4.1 copy-start.76
  408.6 4.1 copy-start.78
  408.7 4.1 copy-start.80
  412.8 4.3 copy-start.11
  412.8 4.3 copy-start.32
  (44 other events, 105.7 us)
Sparse Core Ops, SparseCore 0:
  21.8 32.0 all-gather.1
where the time goes:
time: 446 us; the launch traced here: 442 us
  blocking collectives  219 us (49%)
  local copies, waits for them, and re-layouts  86.1 us (19%)
  matrix products  83.3 us (19%)
  other arithmetic  38.6 us (9%)
  between operations  15 us (3%)
    all_gather x16, blocking collectives, carried_in(): pieces = jax.tree.map(lambda part: lax.all_gather(part, axis), total)  169 us
    dot_general x12, matrix products, project(): return jnp.dot(normed, weight, preferred_element_type=jnp.float32)  29.5 us
    psum x2, blocking collectives, by_axis(): x = lax.psum(x, axis)  21.3 us
    dot_general x2, matrix products, carried_states(): carried = jnp.einsum('nmha,mhae->nhae', weights, summary, precision=highest)  17 us
    all_gather x1, blocking collectives, gather_axes(): nearer = lax.all_gather(x, axes[-1], axis=dim, tiled=True)  15.1 us
    all_gather x1, blocking collectives, in_one_piece(): lax.all_gather(both, axis, axis=dim, tiled=True)  13.3 us
    mul x1, local copies, waits for them, and re-layouts, shards(): query_rows.astype(jnp.float32).reshape(row_count, HEADS, DK) * DK ** (-0.5)  13.2 us
    dot_general x2, matrix products, block_terms(): jnp.einsum('ntha,nsha->nhts', q_decayed, k_decayed, precision=highest)  12 us
  transfers between devices with their start and end apart: 1, of which 0 were waited for; matrix products, arithmetic and copies ran while one was open for 32% of the time, Pallas kernels for 0%

commit v1 on v0

v1 whole, which is shorter than its diff:
```python
import jax
import jax.numpy as jnp
from jax import lax
from jax.experimental import pallas as pl
from jax.experimental.pallas import tpu as pltpu
from jax.sharding import PartitionSpec as P

F32 = jnp.float32
BF16 = jnp.bfloat16
MESH = pl.DeviceIdType.MESH
EPS = 1e-06

NSP = 16
NTP = 8
D = 2048
HEADS = 16
DK = 32
DV = 64
ROWS = 256
CROWS = 32
ALL = ROWS + CROWS
T = 64
NB = ROWS // T
NG = 4
MSG = 80

LOCAL = ("down", "key", "value", "query", "outgate", "out")


def dot(a, b):
    return jnp.dot(a, b, preferred_element_type=F32)


def dot_dims(a, b, ca, cb):
    return lax.dot_general(a, b, (((ca,), (cb,)), ((), ())), preferred_element_type=F32)


def iota(shape, dim):
    return lax.broadcasted_iota(jnp.int32, shape, dim)


def split3(x):
    hi = x.astype(BF16)
    rest = x - hi.astype(F32)
    mid = rest.astype(BF16)
    return hi, mid, (rest - mid.astype(F32)).astype(BF16)


def sum_rows(tri, x):
    hi, mid, lo = split3(x)
    return dot(tri, hi) + dot(tri, mid) + dot(tri, lo)


def log_decays(pre):
    return (jnp.minimum(pre, 0.0) - jnp.log1p(jnp.exp(-jnp.abs(pre)))) * (1.0 / 16.0)


def put_message(ref, at, state, total):
    hi, mid, lo = split3(total)
    row = iota((16, 128), 0)
    tail = jnp.where(
        row == 0,
        hi.astype(F32),
        jnp.where(row == 1, mid.astype(F32), jnp.where(row == 2, lo.astype(F32), 0.0)),
    )
    ref[at, 0:64, :] = state.astype(BF16)
    ref[at, 64:MSG, :] = tail.astype(BF16)


def get_message(ref, at):
    state = ref[at, 0:64, :].astype(F32)
    tail = ref[at, 64:MSG, :].astype(F32)
    return state, tail[0:1] + tail[1:2] + tail[2:3]


def kernel(
    latent,
    context,
    lat_cond,
    ctx_cond,
    shift_w,
    scale_w,
    gate_w,
    gain,
    query_w,
    key_w,
    value_w,
    outgate_w,
    down_w,
    up_w,
    bias,
    out_w,
    post_gain,
    out,
    s,
):
    sp = lax.axis_index("sp")
    tp = lax.axis_index("tp")

    def sp_peer(d):
        return lax.rem(sp + d, NSP)

    def tp_peer(d):
        return lax.rem(tp + d, NTP)

    barrier = pltpu.get_barrier_semaphore()
    for d in range(1, NSP):
        pl.semaphore_signal(barrier, inc=1, device_id=(sp_peer(d), tp), device_id_type=MESH)
    for d in range(1, NTP):
        pl.semaphore_signal(barrier, inc=1, device_id=(sp, tp_peer(d)), device_id_type=MESH)

    pairs = dict(
        latent=(latent, s["lat"]),
        context=(context, s["ctx"]),
        down=(down_w, s["wd"]),
        key=(key_w, s["wk"]),
        value=(value_w, s["wv"]),
        query=(query_w, s["wq"]),
        outgate=(outgate_w, s["wg"]),
        out=(out_w, s["wo"]),
    )
    loads = {
        name: pltpu.make_async_copy(src, dst, s["load_sem"].at[i])
        for i, (name, (src, dst)) in enumerate(pairs.items())
    }
    for name in loads:
        loads[name].start()

    sends = []

    def exchange(axis, src, dst, send_sem, recv_sem):
        n, peer = (NSP, sp_peer) if axis == "sp" else (NTP, tp_peer)
        for d in range(1, n):
            to = peer(d)
            copy = pltpu.make_async_remote_copy(
                src_ref=src(to),
                dst_ref=dst(sp if axis == "sp" else tp),
                send_sem=send_sem.at[d - 1],
                recv_sem=recv_sem.at[d - 1],
                device_id=(to, tp) if axis == "sp" else (sp, to),
                device_id_type=MESH,
            )
            copy.start()
            sends.append(copy)

    def arrive(axis, dst, send_sem, recv_sem):
        n, peer = (NSP, sp_peer) if axis == "sp" else (NTP, tp_peer)
        for d in range(1, n):
            origin = peer(n - d)
            pltpu.make_async_remote_copy(
                src_ref=dst(origin),
                dst_ref=dst(origin),
                send_sem=send_sem.at[d - 1],
                recv_sem=recv_sem.at[d - 1],
                device_id=(origin, tp) if axis == "sp" else (sp, origin),
                device_id_type=MESH,
            ).wait_recv()

    cols = pl.ds(pl.multiple_of(sp * 128, 128), 128)
    parity = lax.rem(iota((16, 128), 0), 2)
    cond = jnp.where(
        parity == 0,
        jnp.broadcast_to(lat_cond[:, cols].astype(F32), (16, 128)),
        jnp.broadcast_to(ctx_cond[:, cols].astype(F32), (16, 128)),
    )
    act = (cond * lax.logistic(cond)).astype(BF16)
    row8 = iota((8, 256), 0)
    part = jnp.where(
        row8 < 2,
        dot(act, shift_w[...])[0:8],
        jnp.where(row8 < 4, dot(act, scale_w[...])[0:8], dot(act, gate_w[...])[0:8]),
    )
    mod1, mod2 = s["mod1"], s["mod2"]
    mod1[sp] = part
    pl.semaphore_wait(barrier, NSP + NTP - 2)
    exchange("sp", lambda to: mod1.at[sp], lambda i: mod1.at[i], s["m1s"], s["m1r"])

    head128, head256, tri, ones = s["head128"], s["head256"], s["tri"], s["ones"]

    def as_bf16(cond):
        return jnp.where(cond, 1.0, 0.0).astype(BF16)

    head128[...] = as_bf16(iota((256, 128), 0) // 64 == iota((256, 128), 1) // 32)
    head256[...] = as_bf16(iota((256, 256), 0) // 64 == iota((256, 256), 1) // 64)
    r256, c256 = iota((256, 256), 0), iota((256, 256), 1)
    tri[...] = as_bf16((r256 // T == c256 // T) & (c256 <= r256))

    arrive("sp", lambda i: mod1.at[i], s["m1s"], s["m1r"])
    total = mod1[0]
    for i in range(1, NSP):
        total = total + mod1[i]
    mod2[tp] = total
    exchange("tp", lambda to: mod2.at[tp], lambda i: mod2.at[i], s["m2s"], s["m2r"])
    loads["latent"].wait()
    loads["context"].wait()
    arrive("tp", lambda i: mod2.at[i], s["m2s"], s["m2r"])
    modv = s["modv"]
    for j in range(NTP):
        modv[:, j * 256 : (j + 1) * 256] = mod2[j]

    lat, ctx, normed = s["lat"], s["ctx"], s["normed"]

    def norm_rows(x, row):
        x = x.astype(F32)
        factor = lax.rsqrt(jnp.mean(x * x, axis=-1, keepdims=True) + EPS)
        scaled = x * factor * gain[...] * (1.0 + modv[2 + row : 3 + row, :])
        return (scaled + modv[row : row + 1, :]).astype(BF16)

    @pl.loop(0, ROWS // 16)
    def _(i):
        at = pl.ds(pl.multiple_of(i * 16, 16), 16)
        normed[at, :] = norm_rows(lat[at, :], 0)

    @pl.loop(0, CROWS // 16)
    def _(i):
        at = pl.multiple_of(i * 16, 16)
        normed[pl.ds(ROWS + at, 16), :] = norm_rows(ctx[pl.ds(at, 16), :], 1)

    ld, lcum, kk, vv = s["ld"], s["lcum"], s["kk"], s["vv"]
    loads["down"].wait()
    low = dot(normed[...], s["wd"][...]).astype(BF16)
    ld[...] = log_decays(dot(low, up_w[...]) + bias[...])
    lcum[0:ROWS, :] = sum_rows(tri[...], ld[0:ROWS, :])
    lcum[ROWS:ALL, :] = sum_rows(tri[0:CROWS, 0:CROWS], ld[ROWS:ALL, :])
    loads["key"].wait()
    kk[...] = dot(normed[...], s["wk"][...]).astype(BF16)
    loads["value"].wait()

    @pl.loop(0, 2)
    def _(c):
        at = pl.ds(pl.multiple_of(c * 512, 512), 512)
        vv[:, at] = dot(normed[...], s["wv"][:, at]).astype(BF16)

    lane_head = lax.rem(iota((64, 256), 1), 128) // 32
    summ, ent, tots = s["summ"], s["ent"], s["tots"]

    def summaries(rows, count, at):
        cum = lcum[rows, :]
        before = cum - ld[rows, :]
        closing = cum[count - 1 : count, :]
        keys = kk[rows, :].astype(F32)
        key_f = (keys * jnp.exp(closing - cum)).astype(BF16)
        key_b = (keys * jnp.exp(before)).astype(BF16)
        for g in range(NG):
            k_at = slice(g * 128, (g + 1) * 128)
            both = jnp.concatenate([key_f[:, k_at], key_b[:, k_at]], axis=1)
            full = dot_dims(vv[rows, g * 256 : (g + 1) * 256], both, 0, 0)
            state = jnp.zeros((64, 256), F32)
            for h in range(4):
                state = jnp.where(lane_head == h, full[h * 64 : (h + 1) * 64], state)
            summ[at, :, g * 256 : (g + 1) * 256] = state

    summaries(slice(ROWS, ALL), CROWS, NB)
    ctx_msg, seg_msg = s["ctx_msg"], s["seg_msg"]
    ctx_all, recv_a, grp_all, back, recv_c = (
        s["ctx_all"],
        s["recv_a"],
        s["grp_all"],
        s["back"],
        s["recv_c"],
    )
    ctx_total = lcum[ALL - 8 : ALL, :][7:8]
    for g in range(NG):
        for d in range(2):
            at = slice(g * 256 + d * 128, g * 256 + (d + 1) * 128)
            put_message(
                ctx_msg, d * NG + g, summ[NB, :, at], ctx_total[:, g * 128 : (g + 1) * 128]
            )
    ctx_all[sp] = ctx_msg[tp]
    exchange("sp", lambda to: ctx_all.at[sp], lambda i: ctx_all.at[i], s["cs"], s["cr"])

    @pl.loop(0, NB)
    def _(n):
        summaries(pl.ds(pl.multiple_of(n * T, T), T), T, n)

    closings = [lcum[n * T + T - 8 : n * T + T, :][7:8] for n in range(NB)]
    for n in range(NB):
        tots[n : n + 1, :] = closings[n]
    for g in range(NG):
        k_at = slice(g * 128, (g + 1) * 128)
        close = [c[:, k_at] for c in closings]
        whole = close[0] + close[1] + close[2] + close[3]
        for d in range(2):
            at = slice(g * 256 + d * 128, g * 256 + (d + 1) * 128)
            run = jnp.zeros((64, 128), F32)
            for n in range(NB) if d == 0 else reversed(range(NB)):
                ent[n, :, at] = run.astype(BF16)
                run = jnp.exp(close[n]) * run + summ[n, :, at]
            put_message(seg_msg, d * NG + g, run, whole)
    recv_a[tp] = seg_msg[tp]
    exchange("tp", lambda to: seg_msg.at[to], lambda i: recv_a.at[i], s["as"], s["ar"])

    qq, gg = s["qq"], s["gg"]
    loads["query"].wait()
    qq[...] = dot(normed[0:ROWS, :], s["wq"][...]).astype(BF16)

    flip = lax.div(tp, NTP // 2)
    arrive("tp", lambda i: recv_a.at[i], s["as"], s["ar"])
    pre_s, pre_c = s["pre_s"], s["pre_c"]
    run = jnp.zeros((64, 128), F32)
    run_log = jnp.zeros((1, 128), F32)
    for i in range(NTP):
        at = i + flip * (NTP - 1 - 2 * i)
        pre_s[at] = run
        pre_c[at] = jnp.broadcast_to(run_log, (8, 128))
        state, total = get_message(recv_a, at)
        run = jnp.exp(total) * run + state
        run_log = run_log + total
    put_message(grp_all, sp, run, run_log)
    exchange("sp", lambda to: grp_all.at[sp], lambda i: grp_all.at[i], s["gs"], s["gr"])

    loads["outgate"].wait()

    @pl.loop(0, 2)
    def _(c):
        at = pl.ds(pl.multiple_of(c * 512, 512), 512)
        gg[:, at] = dot(normed[0:ROWS, :], s["wg"][:, at]).astype(BF16)

    mixed, qd = s["mixed"], s["qd"]
    t_row = iota((64, 256), 0)
    s_col = lax.rem(iota((64, 256), 1), 64)
    up_to, from_on = s_col <= t_row, s_col >= t_row

    def four(x, mask):
        return jnp.concatenate([x, x, x, x], axis=0) * mask

    @pl.loop(0, NB)
    def _(n):
        rows = pl.ds(pl.multiple_of(n * T, T), T)
        cum = lcum[rows, :]
        before = cum - ld[rows, :]
        middle, closing = cum[T // 2 - 1 : T // 2, :], cum[T - 1 : T, :]
        ahead = jnp.zeros((1, 512), F32)
        behind = jnp.zeros((1, 512), F32)
        for m in range(NB):
            ahead = ahead + jnp.where(m < n, tots[m : m + 1, :], 0.0)
            behind = behind + jnp.where(m > n, tots[m : m + 1, :], 0.0)
        q = qq[rows, :].astype(F32) * DK**-0.5
        k = kk[rows, :].astype(F32)
        qm_f = (q * jnp.exp(cum - middle)).astype(BF16)
        qm_b = (q * jnp.exp(middle - before)).astype(BF16)
        km_f = (k * jnp.exp(middle - cum)).astype(BF16)
        km_b = (k * jnp.exp(before - middle)).astype(BF16)
        qs_f = (q * jnp.exp(cum)).astype(BF16)
        qs_b = (q * jnp.exp(closing - before)).astype(BF16)
        qd_f = (q * jnp.exp(cum + ahead)).astype(BF16)
        qd_b = (q * jnp.exp(closing - before + behind)).astype(BF16)
        for g in range(NG):
            k_at = slice(g * 128, (g + 1) * 128)
            v_at = slice(g * 256, (g + 1) * 256)
            qd[rows, v_at] = jnp.concatenate([qd_f[:, k_at], qd_b[:, k_at]], axis=1)
            score_f = dot_dims(qm_f[:, k_at], four(km_f[:, k_at], head128[...]), 1, 1)
            score_b = dot_dims(qm_b[:, k_at], four(km_b[:, k_at], head128[...]), 1, 1)
            score = jnp.where(up_to, score_f, 0.0) + jnp.where(from_on, score_b, 0.0)
            within = dot(score.astype(BF16), four(vv[rows, v_at], head256[...]))
            entering = ent[n, :, v_at]
            states = jnp.concatenate(
                [
                    four(entering[:, 0:128], head128[...]),
                    four(entering[:, 128:256], head128[...]),
                ],
                axis=1,
            )
            across = dot_dims(
                jnp.concatenate([qs_f[:, k_at], qs_b[:, k_at]], axis=1), states, 1, 1
            )
            mixed[rows, v_at] = within + across

    arrive("sp", lambda i: ctx_all.at[i], s["cs"], s["cr"])
    arrive("sp", lambda i: grp_all.at[i], s["gs"], s["gr"])
    reach = jnp.zeros((64, 128), F32)
    for i in range(NSP):
        state, total = get_message(ctx_all, i + flip * (NSP - 1 - 2 * i))
        reach = jnp.exp(total) * reach + state
    rank = sp + flip * (NSP - 1 - 2 * sp)
    for i in range(NSP):
        state, total = get_message(grp_all, i + flip * (NSP - 1 - 2 * i))
        reach = jnp.where(i < rank, jnp.exp(total) * reach + state, reach)
    for j in range(NTP):
        back[j] = (pre_s[j] + jnp.exp(pre_c[j][0:1]) * reach).astype(BF16)
    recv_c[tp] = back[tp]
    exchange("tp", lambda to: back.at[to], lambda i: recv_c.at[i], s["bs"], s["br"])
    ones[...] = head256[...]
    arrive("tp", lambda i: recv_c.at[i], s["bs"], s["br"])

    gated = s["gated"]
    for g in range(NG):
        v_at = slice(g * 256, (g + 1) * 256)
        states = jnp.concatenate(
            [four(recv_c[g], head128[...]), four(recv_c[NG + g], head128[...])], axis=1
        )
        values = mixed[:, v_at] + dot_dims(qd[:, v_at], states, 1, 1)
        square = values * values
        hi = square.astype(BF16)
        low = (square - hi.astype(F32)).astype(BF16)
        power = dot(hi, ones[...]) + dot(low, ones[...])
        gate = gg[:, v_at].astype(F32)
        normal = values * lax.rsqrt(power * (1.0 / DV) + EPS)
        gated[:, v_at] = (normal * (gate * lax.logistic(gate))).astype(BF16)

    branch = s["branch"]
    loads["out"].wait()

    @pl.loop(0, 4)
    def _(c):
        at = pl.ds(pl.multiple_of(c * 512, 512), 512)
        branch[:, at] = dot(gated[...], s["wo"][:, at]).astype(BF16)

    @pl.loop(0, ROWS // 16)
    def _(i):
        at = pl.ds(pl.multiple_of(i * 16, 16), 16)
        b = branch[at, :].astype(F32)
        factor = lax.rsqrt(jnp.mean(b * b, axis=-1, keepdims=True) + EPS)
        added = modv[4:5, :] * (b * factor) * post_gain[...]
        out[at, :] = (lat[at, :].astype(F32) + added).astype(BF16)

    for copy in sends:
        copy.wait_send()


def scratch():
    vmem, sems = pltpu.VMEM, pltpu.SemaphoreType.DMA
    return dict(
        lat=vmem((ROWS, D), BF16),
        ctx=vmem((CROWS, D), BF16),
        wd=vmem((D, 32), BF16),
        wk=vmem((D, 512), BF16),
        wv=vmem((D, 1024), BF16),
        wq=vmem((D, 512), BF16),
        wg=vmem((D, 1024), BF16),
        wo=vmem((1024, D), BF16),
        mod1=vmem((NSP, 8, 256), F32),
        mod2=vmem((NTP, 8, 256), F32),
        modv=vmem((8, D), F32),
        normed=vmem((ALL, D), BF16),
        head128=vmem((256, 128), BF16),
        head256=vmem((256, 256), BF16),
        ones=vmem((256, 256), BF16),
        tri=vmem((256, 256), BF16),
        ld=vmem((ALL, 512), F32),
        lcum=vmem((ALL, 512), F32),
        kk=vmem((ALL, 512), BF16),
        vv=vmem((ALL, 1024), BF16),
        qq=vmem((ROWS, 512), BF16),
        gg=vmem((ROWS, 1024), BF16),
        summ=vmem((NB + 1, 64, 1024), F32),
        ent=vmem((NB, 64, 1024), BF16),
        tots=vmem((8, 512), F32),
        ctx_msg=vmem((NTP, MSG, 128), BF16),
        seg_msg=vmem((NTP, MSG, 128), BF16),
        ctx_all=vmem((NSP, MSG, 128), BF16),
        grp_all=vmem((NSP, MSG, 128), BF16),
        recv_a=vmem((NTP, MSG, 128), BF16),
        pre_s=vmem((NTP, 64, 128), F32),
        pre_c=vmem((NTP, 8, 128), F32),
        back=vmem((NTP, 64, 128), BF16),
        recv_c=vmem((NTP, 64, 128), BF16),
        mixed=vmem((ROWS, 1024), F32),
        qd=vmem((ROWS, 1024), BF16),
        gated=vmem((ROWS, 1024), BF16),
        branch=vmem((ROWS, D), BF16),
        load_sem=sems((8,)),
        m1s=sems((NSP - 1,)),
        m1r=sems((NSP - 1,)),
        m2s=sems((NTP - 1,)),
        m2r=sems((NTP - 1,)),
        cs=sems((NSP - 1,)),
        cr=sems((NSP - 1,)),
        gs=sems((NSP - 1,)),
        gr=sems((NSP - 1,)),
        bs=sems((NTP - 1,)),
        br=sems((NTP - 1,)),
        **{"as": sems((NTP - 1,)), "ar": sems((NTP - 1,))},
    )


def shards(
    latent,
    context,
    latent_condition,
    context_condition,
    shift_weight,
    scale_weight,
    gate_weight,
    norm_gain,
    query_weight,
    key_weight,
    value_weight,
    outgate_weight,
    down_weight,
    up_weight,
    decay_bias,
    out_weight,
    post_gain,
):
    spaces = "hhvvvvvvhhhhhvvhv"
    specs = [
        pl.BlockSpec(memory_space=pltpu.VMEM if c == "v" else pl.ANY) for c in spaces
    ]
    return pl.pallas_call(
        kernel,
        out_shape=jax.ShapeDtypeStruct((ROWS, D), BF16),
        in_specs=specs,
        out_specs=pl.BlockSpec(memory_space=pltpu.VMEM),
        scratch_shapes=[scratch()],
        compiler_params=pltpu.CompilerParams(
            collective_id=0, has_side_effects=True, vmem_limit_bytes=60 * 1024 * 1024
        ),
    )(
        latent,
        context,
        latent_condition[None],
        context_condition[None],
        shift_weight,
        scale_weight,
        gate_weight,
        norm_gain[None],
        query_weight,
        key_weight,
        value_weight,
        outgate_weight,
        down_weight,
        up_weight,
        decay_bias[None],
        out_weight,
        post_gain[None],
    )


def solution(mesh):
    tokens = P(("sp", "tp"), None)
    maps = P("sp", "tp")
    placed = (tokens, P("sp", None), P(), P(), maps, maps, maps) + (P(),) * 10
    return jax.shard_map(
        shards, mesh=mesh, in_specs=placed, out_specs=tokens, check_vma=False
    )
```

time: 446 us -> 55.6 us (0.12)
  the two profiles are of different devices: /device:TPU:0 before, /device:TPU:1 now
where the time goes in v1:
time: 55.6 us; the launch traced here: 55.4 us
  Pallas kernels  48.6 us (87%)
  local copies, waits for them, and re-layouts  6.78 us (12%)
    pallas_call x1, Pallas kernels, shards(): pl.pallas_call(kernel, out_shape=jax.ShapeDtypeStruct((ROWS, D), BF16), i...  48.6 us
    unnamed x2, local copies, waits for them, and re-layouts  4.21 us
    broadcast_in_dim x1, local copies, waits for them, and re-layouts, shards(): context_condition[None]  1.29 us
    broadcast_in_dim x1, local copies, waits for them, and re-layouts, shards(): latent_condition[None]  1.28 us

profile of v1, /device:TPU:1, one launch (start us, length us, event | category | flops | bytes accessed | tf_op | source)
XLA Modules:
  0.0 55.4 jit_solution(12982046613501376065)
XLA Ops:
  0.0 1.3 %broadcast_in_dim.15.lat_cond = bf16[1,2048]{1,0:T(2,128)(2,1)} reshape(bf16[2048]{0:T(1024)(128)(2,1)} %param.19) | data formatting | bytes 8192 | tf_op jit(solution)/shard_map/broadcast_in_dim | solution.py:512
  1.3 1.3 %broadcast_in_dim.16.ctx_cond = bf16[1,2048]{1,0:T(2,128)(2,1)} reshape(bf16[2048]{0:T(1024)(128)(2,1)} %param.20) | data formatting | bytes 8192 | tf_op jit(solution)/shard_map/broadcast_in_dim | solution.py:513
  2.6 1.9 %copy.18.down_w = bf16[2048,32]{1,0:T(8,128)(2,1)} copy(bf16[2048,32]{0,1:T(8,128)(2,1)} %param.29) | data formatting | bytes 262144 | tf_op args[12]
  4.5 48.6 %shard_map.163 = bf16[256,2048]{1,0:T(8,128)(2,1)} custom-call(bf16[256,2048]{1,0:T(8,128)(2,1)} %latent.1, bf16[32,2048]{1,0:T(8,128)(2,1)} %context.1, bf16[1,2048]{1,0:T(2,128)(2,1)} %broadcast_in_dim.15.lat_cond, bf16[1,2048]{1,0:T(2,128)(2,1)} %broadcast_in_dim.16.ctx_cond, bf16[128,256]{1,0:T(8,128)(2,1)} %shift_w.1, bf16[128,256]{1,0:T(8,128)(2,1)} %scale_w.1, ...), custom_call_target="tpu_custom_call" | custom-call | tf_op jit(solution)/shard_map/pallas_call | solution.py:500
  53.1 2.3 %copy.20 = bf16[256,2048]{1,0:T(8,128)(2,1)} copy(bf16[256,2048]{1,0:T(8,128)(2,1)} %shard_map.163) | data formatting | bytes 2097152

commit v2 on v1

--- a/solution.py
+++ b/solution.py
@@ -24,7 +24,16 @@
 NG = 4
 MSG = 80
 
-LOCAL = ("down", "key", "value", "query", "outgate", "out")
+
+def far_first(lengths):
+    steps = [(a, b) for a in range(lengths[0]) for b in range(lengths[1]) if (a, b) != (0, 0)]
+    hops = [0, 1, 2, 1]
+    weight = 2 if lengths[1] == 2 else 1
+    return sorted(steps, key=lambda t: -(weight * hops[t[0]] + hops[t[1]]))
+
+
+SP_STEPS = far_first((4, 4))
+TP_STEPS = far_first((4, 2))
 
 
 def dot(a, b):
@@ -97,21 +106,33 @@
     sp = lax.axis_index("sp")
     tp = lax.axis_index("tp")
 
-    def sp_peer(d):
-        return lax.rem(sp + d, NSP)
-
-    def tp_peer(d):
-        return lax.rem(tp + d, NTP)
+    z, x = lax.div(sp, 4), lax.rem(sp, 4)
+    y, c = lax.div(tp, 2), lax.rem(tp, 2)
+
+    def sp_peer(step):
+        return lax.rem(z + step[0], 4) * 4 + lax.rem(x + step[1], 4)
+
+    def tp_peer(step):
+        return lax.rem(y + step[0], 4) * 2 + lax.rem(c + step[1], 2)
 
     barrier = pltpu.get_barrier_semaphore()
-    for d in range(1, NSP):
-        pl.semaphore_signal(barrier, inc=1, device_id=(sp_peer(d), tp), device_id_type=MESH)
-    for d in range(1, NTP):
-        pl.semaphore_signal(barrier, inc=1, device_id=(sp, tp_peer(d)), device_id_type=MESH)
+    for step in SP_STEPS:
+        pl.semaphore_signal(barrier, inc=1, device_id=(sp_peer(step), tp), device_id_type=MESH)
+    for step in TP_STEPS:
+        pl.semaphore_signal(barrier, inc=1, device_id=(sp, tp_peer(step)), device_id_type=MESH)
 
     pairs = dict(
+        lat_cond=(lat_cond, s["lat_cond"]),
+        ctx_cond=(ctx_cond, s["ctx_cond"]),
+        shift=(shift_w, s["shift_w"]),
+        scale=(scale_w, s["scale_w"]),
+        gate=(gate_w, s["gate_w"]),
         latent=(latent, s["lat"]),
         context=(context, s["ctx"]),
+        gain=(gain, s["gain"]),
+        bias=(bias, s["bias"]),
+        up=(up_w, s["up_w"]),
+        post=(post_gain, s["post_gain"]),
         down=(down_w, s["wd"]),
         key=(key_w, s["wk"]),
         value=(value_w, s["wv"]),
@@ -126,17 +147,21 @@
     for name in loads:
         loads[name].start()
 
+    def loaded(*names):
+        for name in names:
+            loads[name].wait()
+
     sends = []
 
     def exchange(axis, src, dst, send_sem, recv_sem):
-        n, peer = (NSP, sp_peer) if axis == "sp" else (NTP, tp_peer)
-        for d in range(1, n):
-            to = peer(d)
+        steps, peer = (SP_STEPS, sp_peer) if axis == "sp" else (TP_STEPS, tp_peer)
+        for d, step in enumerate(steps):
+            to = peer(step)
             copy = pltpu.make_async_remote_copy(
                 src_ref=src(to),
                 dst_ref=dst(sp if axis == "sp" else tp),
-                send_sem=send_sem.at[d - 1],
-                recv_sem=recv_sem.at[d - 1],
+                send_sem=send_sem.at[d],
+                recv_sem=recv_sem.at[d],
                 device_id=(to, tp) if axis == "sp" else (sp, to),
                 device_id_type=MESH,
             )
@@ -144,31 +169,34 @@
             sends.append(copy)
 
     def arrive(axis, dst, send_sem, recv_sem):
-        n, peer = (NSP, sp_peer) if axis == "sp" else (NTP, tp_peer)
-        for d in range(1, n):
-            origin = peer(n - d)
+        steps, wrap, peer = (
+            (SP_STEPS, (4, 4), sp_peer) if axis == "sp" else (TP_STEPS, (4, 2), tp_peer)
+        )
+        for d, step in reversed(list(enumerate(steps))):
+            origin = peer((wrap[0] - step[0], wrap[1] - step[1]))
             pltpu.make_async_remote_copy(
                 src_ref=dst(origin),
                 dst_ref=dst(origin),
-                send_sem=send_sem.at[d - 1],
-                recv_sem=recv_sem.at[d - 1],
+                send_sem=send_sem.at[d],
+                recv_sem=recv_sem.at[d],
                 device_id=(origin, tp) if axis == "sp" else (sp, origin),
                 device_id_type=MESH,
             ).wait_recv()
 
-    cols = pl.ds(pl.multiple_of(sp * 128, 128), 128)
-    parity = lax.rem(iota((16, 128), 0), 2)
-    cond = jnp.where(
-        parity == 0,
-        jnp.broadcast_to(lat_cond[:, cols].astype(F32), (16, 128)),
-        jnp.broadcast_to(ctx_cond[:, cols].astype(F32), (16, 128)),
-    )
+    loaded("lat_cond", "ctx_cond", "shift", "scale", "gate")
+    row16 = iota((16, 128), 0)
+
+    def cond_row(name):
+        mine = jnp.where(row16 == sp, s[name][...].astype(F32), 0.0)
+        return jnp.broadcast_to(jnp.sum(mine, axis=0, keepdims=True), (16, 128))
+
+    cond = jnp.where(lax.rem(row16, 2) == 0, cond_row("lat_cond"), cond_row("ctx_cond"))
     act = (cond * lax.logistic(cond)).astype(BF16)
     row8 = iota((8, 256), 0)
     part = jnp.where(
         row8 < 2,
-        dot(act, shift_w[...])[0:8],
-        jnp.where(row8 < 4, dot(act, scale_w[...])[0:8], dot(act, gate_w[...])[0:8]),
+        dot(act, s["shift_w"][...])[0:8],
+        jnp.where(row8 < 4, dot(act, s["scale_w"][...])[0:8], dot(act, s["gate_w"][...])[0:8]),
     )
     mod1, mod2 = s["mod1"], s["mod2"]
     mod1[sp] = part
@@ -184,6 +212,26 @@
     head256[...] = as_bf16(iota((256, 256), 0) // 64 == iota((256, 256), 1) // 64)
     r256, c256 = iota((256, 256), 0), iota((256, 256), 1)
     tri[...] = as_bf16((r256 // T == c256 // T) & (c256 <= r256))
+
+    lat, ctx, normed, ready = s["lat"], s["ctx"], s["normed"], s["ready"]
+    gain_row = s["gain"]
+
+    def norm_rows(x):
+        x = x.astype(F32)
+        factor = lax.rsqrt(jnp.mean(x * x, axis=-1, keepdims=True) + EPS)
+        return x * factor * gain_row[...]
+
+    loaded("latent", "context", "gain")
+
+    @pl.loop(0, CROWS // 16)
+    def _(i):
+        at = pl.multiple_of(i * 16, 16)
+        ready[pl.ds(ROWS + at, 16), :] = norm_rows(ctx[pl.ds(at, 16), :])
+
+    @pl.loop(0, ROWS // 16)
+    def _(i):
+        at = pl.ds(pl.multiple_of(i * 16, 16), 16)
+        ready[at, :] = norm_rows(lat[at, :])
 
     arrive("sp", lambda i: mod1.at[i], s["m1s"], s["m1r"])
     total = mod1[0]
@@ -191,40 +239,29 @@
         total = total + mod1[i]
     mod2[tp] = total
     exchange("tp", lambda to: mod2.at[tp], lambda i: mod2.at[i], s["m2s"], s["m2r"])
-    loads["latent"].wait()
-    loads["context"].wait()
     arrive("tp", lambda i: mod2.at[i], s["m2s"], s["m2r"])
     modv = s["modv"]
     for j in range(NTP):
         modv[:, j * 256 : (j + 1) * 256] = mod2[j]
 
-    lat, ctx, normed = s["lat"], s["ctx"], s["normed"]
-
-    def norm_rows(x, row):
-        x = x.astype(F32)
-        factor = lax.rsqrt(jnp.mean(x * x, axis=-1, keepdims=True) + EPS)
-        scaled = x * factor * gain[...] * (1.0 + modv[2 + row : 3 + row, :])
-        return (scaled + modv[row : row + 1, :]).astype(BF16)
-
-    @pl.loop(0, ROWS // 16)
+    loaded("bias", "up", "post", "down", "key", "value", "query", "outgate", "out")
+
+    def modulated(at, row):
+        scaled = ready[at, :] * (1.0 + modv[2 + row : 3 + row, :])
+        normed[at, :] = (scaled + modv[row : row + 1, :]).astype(BF16)
+
+    @pl.loop(0, ROWS // 32)
     def _(i):
-        at = pl.ds(pl.multiple_of(i * 16, 16), 16)
-        normed[at, :] = norm_rows(lat[at, :], 0)
-
-    @pl.loop(0, CROWS // 16)
-    def _(i):
-        at = pl.multiple_of(i * 16, 16)
-        normed[pl.ds(ROWS + at, 16), :] = norm_rows(ctx[pl.ds(at, 16), :], 1)
+        modulated(pl.ds(pl.multiple_of(i * 32, 32), 32), 0)
+
+    modulated(pl.ds(ROWS, CROWS), 1)
 
     ld, lcum, kk, vv = s["ld"], s["lcum"], s["kk"], s["vv"]
-    loads["down"].wait()
-    low = dot(normed[...], s["wd"][...]).astype(BF16)
-    ld[...] = log_decays(dot(low, up_w[...]) + bias[...])
+    low = dot_dims(normed[...], s["wd"][...], 1, 1).astype(BF16)
+    ld[...] = log_decays(dot(low, s["up_w"][...]) + s["bias"][...])
     lcum[0:ROWS, :] = sum_rows(tri[...], ld[0:ROWS, :])
     lcum[ROWS:ALL, :] = sum_rows(tri[0:CROWS, 0:CROWS], ld[ROWS:ALL, :])
-    loads["key"].wait()
     kk[...] = dot(normed[...], s["wk"][...]).astype(BF16)
-    loads["value"].wait()
 
     @pl.loop(0, 2)
     def _(c):
@@ -291,7 +328,6 @@
     exchange("tp", lambda to: seg_msg.at[to], lambda i: recv_a.at[i], s["as"], s["ar"])
 
     qq, gg = s["qq"], s["gg"]
-    loads["query"].wait()
     qq[...] = dot(normed[0:ROWS, :], s["wq"][...]).astype(BF16)
 
     flip = lax.div(tp, NTP // 2)
@@ -309,7 +345,6 @@
     put_message(grp_all, sp, run, run_log)
     exchange("sp", lambda to: grp_all.at[sp], lambda i: grp_all.at[i], s["gs"], s["gr"])
 
-    loads["outgate"].wait()
 
     @pl.loop(0, 2)
     def _(c):
@@ -367,11 +402,11 @@
             mixed[rows, v_at] = within + across
 
     arrive("sp", lambda i: ctx_all.at[i], s["cs"], s["cr"])
-    arrive("sp", lambda i: grp_all.at[i], s["gs"], s["gr"])
     reach = jnp.zeros((64, 128), F32)
     for i in range(NSP):
         state, total = get_message(ctx_all, i + flip * (NSP - 1 - 2 * i))
         reach = jnp.exp(total) * reach + state
+    arrive("sp", lambda i: grp_all.at[i], s["gs"], s["gr"])
     rank = sp + flip * (NSP - 1 - 2 * sp)
     for i in range(NSP):
         state, total = get_message(grp_all, i + flip * (NSP - 1 - 2 * i))
@@ -398,21 +433,38 @@
         normal = values * lax.rsqrt(power * (1.0 / DV) + EPS)
         gated[:, v_at] = (normal * (gate * lax.logistic(gate))).astype(BF16)
 
-    branch = s["branch"]
-    loads["out"].wait()
-
-    @pl.loop(0, 4)
-    def _(c):
-        at = pl.ds(pl.multiple_of(c * 512, 512), 512)
-        branch[:, at] = dot(gated[...], s["wo"][:, at]).astype(BF16)
+    branch, result = s["branch"], s["result"]
+    squares = jnp.zeros((ROWS, 128), F32)
+    for i in range(4):
+        at = slice(i * 512, (i + 1) * 512)
+        part = dot(gated[...], s["wo"][:, at]).astype(BF16)
+        branch[:, at] = part
+        part = part.astype(F32)
+        part = part * part
+        for j in range(4):
+            squares = squares + part[:, j * 128 : (j + 1) * 128]
+    mean = jnp.sum(squares, axis=-1, keepdims=True) * (1.0 / D)
+    s["factor"][...] = jnp.broadcast_to(lax.rsqrt(mean + EPS), (ROWS, 128))
+    weight = s["weight"]
+    weight[...] = jnp.broadcast_to(modv[4:5, :] * s["post_gain"][...], (8, D))
 
     @pl.loop(0, ROWS // 16)
     def _(i):
         at = pl.ds(pl.multiple_of(i * 16, 16), 16)
-        b = branch[at, :].astype(F32)
-        factor = lax.rsqrt(jnp.mean(b * b, axis=-1, keepdims=True) + EPS)
-        added = modv[4:5, :] * (b * factor) * post_gain[...]
-        out[at, :] = (lat[at, :].astype(F32) + added).astype(BF16)
+        factor = s["factor"][at, 0:1]
+        added = branch[at, :].astype(F32) * factor * weight[0:1, :]
+        result[at, :] = (lat[at, :].astype(F32) + added).astype(BF16)
+
+        @pl.when(lax.rem(i, 4) == 3)
+        def _():
+            rows = pl.ds(pl.multiple_of((i - 3) * 16, 64), 64)
+            pltpu.make_async_copy(
+                result.at[rows, :], out.at[rows, :], s["out_sem"].at[lax.div(i, 4)]
+            ).start()
+
+    for i in range(ROWS // 64):
+        rows = pl.ds(i * 64, 64)
+        pltpu.make_async_copy(result.at[rows, :], out.at[rows, :], s["out_sem"].at[i]).wait()
 
     for copy in sends:
         copy.wait_send()
@@ -423,7 +475,7 @@
     return dict(
         lat=vmem((ROWS, D), BF16),
         ctx=vmem((CROWS, D), BF16),
-        wd=vmem((D, 32), BF16),
+        wd=vmem((32, D), BF16),
         wk=vmem((D, 512), BF16),
         wv=vmem((D, 1024), BF16),
         wq=vmem((D, 512), BF16),
@@ -459,7 +511,21 @@
         qd=vmem((ROWS, 1024), BF16),
         gated=vmem((ROWS, 1024), BF16),
         branch=vmem((ROWS, D), BF16),
-        load_sem=sems((8,)),
+        lat_cond=vmem((16, 128), BF16),
+        ctx_cond=vmem((16, 128), BF16),
+        shift_w=vmem((128, 256), BF16),
+        scale_w=vmem((128, 256), BF16),
+        gate_w=vmem((128, 256), BF16),
+        gain=vmem((1, D), F32),
+        bias=vmem((1, 512), F32),
+        up_w=vmem((32, 512), BF16),
+        post_gain=vmem((1, D), F32),
+        ready=vmem((ALL, D), F32),
+        result=vmem((ROWS, D), BF16),
+        factor=vmem((ROWS, 128), F32),
+        weight=vmem((8, D), F32),
+        out_sem=sems((4,)),
+        load_sem=sems((17,)),
         m1s=sems((NSP - 1,)),
         m1r=sems((NSP - 1,)),
         m2s=sems((NTP - 1,)),
@@ -493,15 +559,12 @@
     out_weight,
     post_gain,
 ):
-    spaces = "hhvvvvvvhhhhhvvhv"
-    specs = [
-        pl.BlockSpec(memory_space=pltpu.VMEM if c == "v" else pl.ANY) for c in spaces
-    ]
+    hbm = pl.BlockSpec(memory_space=pl.ANY)
     return pl.pallas_call(
         kernel,
         out_shape=jax.ShapeDtypeStruct((ROWS, D), BF16),
-        in_specs=specs,
-        out_specs=pl.BlockSpec(memory_space=pltpu.VMEM),
+        in_specs=[hbm] * 17,
+        out_specs=hbm,
         scratch_shapes=[scratch()],
         compiler_params=pltpu.CompilerParams(
             collective_id=0, has_side_effects=True, vmem_limit_bytes=60 * 1024 * 1024
@@ -509,8 +572,8 @@
     )(
         latent,
         context,
-        latent_condition[None],
-        context_condition[None],
+        latent_condition.reshape(16, 128),
+        context_condition.reshape(16, 128),
         shift_weight,
         scale_weight,
         gate_weight,
@@ -519,7 +582,7 @@
         key_weight,
         value_weight,
         outgate_weight,
-        down_weight,
+        down_weight.T,
         up_weight,
         decay_bias[None],
         out_weight,

time: 55.6 us -> 45.4 us (0.82)
  Pallas kernels: 48.6 us -> 43 us
  local copies, waits for them, and re-layouts: 6.78 us -> 2.3 us
    pallas_call x1, Pallas kernels: 48.6 us -> 43 us  [shards(): pl.pallas_call(kernel, out_shape=jax.ShapeDtypeStruct((ROWS, D), BF16), i...]
    broadcast_in_dim x2 -> x0, local copies, waits for them, and re-layouts: 2.57 us -> none  [the longest x1 1.29 us: shards(): context_condition[None]]
    unnamed x2 -> x1, local copies, waits for them, and re-layouts: 4.21 us -> 2.3 us
where the time goes in v2:
time: 45.4 us; the launch traced here: 45.3 us
  Pallas kernels  43 us (95%)
  local copies, waits for them, and re-layouts  2.3 us (5%)
    pallas_call x1, Pallas kernels, shards(): pl.pallas_call(kernel, out_shape=jax.ShapeDtypeStruct((ROWS, D), BF16), i...  43 us
    unnamed x1, local copies, waits for them, and re-layouts  2.3 us

profile of v2, /device:TPU:1, one launch (start us, length us, event | category | flops | bytes accessed | tf_op | source)
XLA Modules:
  0.0 45.3 jit_solution(3893433296715877353)
XLA Ops:
  0.0 43.0 %shard_map.163 = bf16[256,2048]{1,0:T(8,128)(2,1)} custom-call(bf16[256,2048]{1,0:T(8,128)(2,1)} %latent.1, bf16[32,2048]{1,0:T(8,128)(2,1)} %context.1, bf16[16,128]{1,0:T(8,128)(2,1)} %bitcast.9, bf16[16,128]{1,0:T(8,128)(2,1)} %bitcast.10, bf16[128,256]{1,0:T(8,128)(2,1)} %shift_w.1, bf16[128,256]{1,0:T(8,128)(2,1)} %scale_w.1, bf16[128,256]{1,0:T(8,128)(2,1)} %gate_w.1, ...), custom_call_target="tpu_custom_call" | custom-call | tf_op jit(solution)/shard_map/pallas_call | solution.py:563
  43.0 2.3 %copy.19 = bf16[256,2048]{1,0:T(8,128)(2,1)} copy(bf16[256,2048]{1,0:T(8,128)(2,1)} %shard_map.163) | data formatting | bytes 2097152

commit v3 on v2

--- a/solution.py
+++ b/solution.py
@@ -257,21 +257,73 @@
     modulated(pl.ds(ROWS, CROWS), 1)
 
     ld, lcum, kk, vv = s["ld"], s["lcum"], s["kk"], s["vv"]
-    low = dot_dims(normed[...], s["wd"][...], 1, 1).astype(BF16)
-    ld[...] = log_decays(dot(low, s["up_w"][...]) + s["bias"][...])
-    lcum[0:ROWS, :] = sum_rows(tri[...], ld[0:ROWS, :])
-    lcum[ROWS:ALL, :] = sum_rows(tri[0:CROWS, 0:CROWS], ld[ROWS:ALL, :])
-    kk[...] = dot(normed[...], s["wk"][...]).astype(BF16)
-
-    @pl.loop(0, 2)
-    def _(c):
-        at = pl.ds(pl.multiple_of(c * 512, 512), 512)
-        vv[:, at] = dot(normed[...], s["wv"][:, at]).astype(BF16)
-
+
+    def project(rows):
+        low = dot_dims(normed[rows, :], s["wd"][...], 1, 1).astype(BF16)
+        ld[rows, :] = log_decays(dot(low, s["up_w"][...]) + s["bias"][...])
+        kk[rows, :] = dot(normed[rows, :], s["wk"][...]).astype(BF16)
+        for i in range(2):
+            at = slice(i * 512, (i + 1) * 512)
+            vv[rows, at] = dot(normed[rows, :], s["wv"][:, at]).astype(BF16)
+
+    own, ctx_rows = slice(0, ROWS), slice(ROWS, ALL)
+    project(own)
+    lcum[own, :] = sum_rows(tri[...], ld[own, :])
+
+    ent, tots, kd = s["ent"], s["tots"], s["kd"]
+    ctx_msg, seg_msg = s["ctx_msg"], s["seg_msg"]
+    ctx_all, recv_a, grp_all, back, recv_c = (
+        s["ctx_all"],
+        s["recv_a"],
+        s["grp_all"],
+        s["back"],
+        s["recv_c"],
+    )
     lane_head = lax.rem(iota((64, 256), 1), 128) // 32
-    summ, ent, tots = s["summ"], s["ent"], s["tots"]
-
-    def summaries(rows, count, at):
+    closings = [lcum[n * T + T - 8 : n * T + T, :][7:8] for n in range(NB)]
+    whole = closings[0] + closings[1] + closings[2] + closings[3]
+
+    def own_lanes(full):
+        state = jnp.zeros((64, 256), F32)
+        for h in range(4):
+            state = jnp.where(lane_head == h, full[h * 64 : (h + 1) * 64], state)
+        return state
+
+    for n in range(NB):
+        tots[n : n + 1, :] = closings[n]
+        rows = slice(n * T, (n + 1) * T)
+        ahead = behind = jnp.zeros((1, 512), F32)
+        for m in range(n):
+            ahead = ahead + closings[m]
+        for m in range(n + 1, NB):
+            behind = behind + closings[m]
+        cum = lcum[rows, :]
+        keys = kk[rows, :].astype(F32)
+        key_f = (keys * jnp.exp(closings[n] - cum + behind)).astype(BF16)
+        key_b = (keys * jnp.exp(cum - ld[rows, :] + ahead)).astype(BF16)
+        for g in range(NG):
+            k_at = slice(g * 128, (g + 1) * 128)
+            kd[rows, g * 256 : (g + 1) * 256] = jnp.concatenate(
+                [key_f[:, k_at], key_b[:, k_at]], axis=1
+            )
+    for g in range(NG):
+        v_at = slice(g * 256, (g + 1) * 256)
+        state = own_lanes(dot_dims(vv[own, v_at], kd[:, v_at], 0, 0))
+        for d in range(2):
+            put_message(
+                seg_msg,
+                d * NG + g,
+                state[:, d * 128 : (d + 1) * 128],
+                whole[:, g * 128 : (g + 1) * 128],
+            )
+    recv_a[tp] = seg_msg[tp]
+    exchange("tp", lambda to: seg_msg.at[to], lambda i: recv_a.at[i], s["as"], s["ar"])
+
+    project(ctx_rows)
+    lcum[ctx_rows, :] = sum_rows(tri[0:CROWS, 0:CROWS], ld[ctx_rows, :])
+    summ = s["summ"]
+
+    def summaries(rows, count, put):
         cum = lcum[rows, :]
         before = cum - ld[rows, :]
         closing = cum[count - 1 : count, :]
@@ -281,54 +333,41 @@
         for g in range(NG):
             k_at = slice(g * 128, (g + 1) * 128)
             both = jnp.concatenate([key_f[:, k_at], key_b[:, k_at]], axis=1)
-            full = dot_dims(vv[rows, g * 256 : (g + 1) * 256], both, 0, 0)
-            state = jnp.zeros((64, 256), F32)
-            for h in range(4):
-                state = jnp.where(lane_head == h, full[h * 64 : (h + 1) * 64], state)
-            summ[at, :, g * 256 : (g + 1) * 256] = state
-
-    summaries(slice(ROWS, ALL), CROWS, NB)
-    ctx_msg, seg_msg = s["ctx_msg"], s["seg_msg"]
-    ctx_all, recv_a, grp_all, back, recv_c = (
-        s["ctx_all"],
-        s["recv_a"],
-        s["grp_all"],
-        s["back"],
-        s["recv_c"],
-    )
+            put(g, own_lanes(dot_dims(vv[rows, g * 256 : (g + 1) * 256], both, 0, 0)))
+
     ctx_total = lcum[ALL - 8 : ALL, :][7:8]
-    for g in range(NG):
+
+    def put_context(g, state):
         for d in range(2):
-            at = slice(g * 256 + d * 128, g * 256 + (d + 1) * 128)
             put_message(
-                ctx_msg, d * NG + g, summ[NB, :, at], ctx_total[:, g * 128 : (g + 1) * 128]
+                ctx_msg,
+                d * NG + g,
+                state[:, d * 128 : (d + 1) * 128],
+                ctx_total[:, g * 128 : (g + 1) * 128],
             )
+
+    summaries(ctx_rows, CROWS, put_context)
     ctx_all[sp] = ctx_msg[tp]
     exchange("sp", lambda to: ctx_all.at[sp], lambda i: ctx_all.at[i], s["cs"], s["cr"])
 
+    qq, gg = s["qq"], s["gg"]
+    qq[...] = dot(normed[0:ROWS, :], s["wq"][...]).astype(BF16)
+
     @pl.loop(0, NB)
     def _(n):
-        summaries(pl.ds(pl.multiple_of(n * T, T), T), T, n)
-
-    closings = [lcum[n * T + T - 8 : n * T + T, :][7:8] for n in range(NB)]
-    for n in range(NB):
-        tots[n : n + 1, :] = closings[n]
+        def put(g, state):
+            summ[n, :, g * 256 : (g + 1) * 256] = state
+
+        summaries(pl.ds(pl.multiple_of(n * T, T), T), T, put)
+
     for g in range(NG):
-        k_at = slice(g * 128, (g + 1) * 128)
-        close = [c[:, k_at] for c in closings]
-        whole = close[0] + close[1] + close[2] + close[3]
+        close = [jnp.exp(tots[n : n + 1, g * 128 : (g + 1) * 128]) for n in range(NB)]
         for d in range(2):
             at = slice(g * 256 + d * 128, g * 256 + (d + 1) * 128)
             run = jnp.zeros((64, 128), F32)
             for n in range(NB) if d == 0 else reversed(range(NB)):
                 ent[n, :, at] = run.astype(BF16)
-                run = jnp.exp(close[n]) * run + summ[n, :, at]
-            put_message(seg_msg, d * NG + g, run, whole)
-    recv_a[tp] = seg_msg[tp]
-    exchange("tp", lambda to: seg_msg.at[to], lambda i: recv_a.at[i], s["as"], s["ar"])
-
-    qq, gg = s["qq"], s["gg"]
-    qq[...] = dot(normed[0:ROWS, :], s["wq"][...]).astype(BF16)
+                run = close[n] * run + summ[n, :, at]
 
     flip = lax.div(tp, NTP // 2)
     arrive("tp", lambda i: recv_a.at[i], s["as"], s["ar"])
@@ -416,6 +455,16 @@
     recv_c[tp] = back[tp]
     exchange("tp", lambda to: back.at[to], lambda i: recv_c.at[i], s["bs"], s["br"])
     ones[...] = head256[...]
+    silu = s["silu"]
+
+    @pl.loop(0, ROWS // 32)
+    def _(i):
+        at = pl.ds(pl.multiple_of(i * 32, 32), 32)
+        gate = gg[at, :].astype(F32)
+        silu[at, :] = gate * lax.logistic(gate)
+
+    weight = s["weight"]
+    weight[...] = jnp.broadcast_to(modv[4:5, :] * s["post_gain"][...], (8, D))
     arrive("tp", lambda i: recv_c.at[i], s["bs"], s["br"])
 
     gated = s["gated"]
@@ -429,11 +478,10 @@
         hi = square.astype(BF16)
         low = (square - hi.astype(F32)).astype(BF16)
         power = dot(hi, ones[...]) + dot(low, ones[...])
-        gate = gg[:, v_at].astype(F32)
         normal = values * lax.rsqrt(power * (1.0 / DV) + EPS)
-        gated[:, v_at] = (normal * (gate * lax.logistic(gate))).astype(BF16)
-
-    branch, result = s["branch"], s["result"]
+        gated[:, v_at] = (normal * silu[:, v_at]).astype(BF16)
+
+    branch = s["branch"]
     squares = jnp.zeros((ROWS, 128), F32)
     for i in range(4):
         at = slice(i * 512, (i + 1) * 512)
@@ -445,26 +493,14 @@
             squares = squares + part[:, j * 128 : (j + 1) * 128]
     mean = jnp.sum(squares, axis=-1, keepdims=True) * (1.0 / D)
     s["factor"][...] = jnp.broadcast_to(lax.rsqrt(mean + EPS), (ROWS, 128))
-    weight = s["weight"]
-    weight[...] = jnp.broadcast_to(modv[4:5, :] * s["post_gain"][...], (8, D))
 
     @pl.loop(0, ROWS // 16)
     def _(i):
         at = pl.ds(pl.multiple_of(i * 16, 16), 16)
         factor = s["factor"][at, 0:1]
         added = branch[at, :].astype(F32) * factor * weight[0:1, :]
-        result[at, :] = (lat[at, :].astype(F32) + added).astype(BF16)
-
-        @pl.when(lax.rem(i, 4) == 3)
-        def _():
-            rows = pl.ds(pl.multiple_of((i - 3) * 16, 64), 64)
-            pltpu.make_async_copy(
-                result.at[rows, :], out.at[rows, :], s["out_sem"].at[lax.div(i, 4)]
-            ).start()
-
-    for i in range(ROWS // 64):
-        rows = pl.ds(i * 64, 64)
-        pltpu.make_async_copy(result.at[rows, :], out.at[rows, :], s["out_sem"].at[i]).wait()
+        out[at, :] = (lat[at, :].astype(F32) + added).astype(BF16)
+
 
     for copy in sends:
         copy.wait_send()
@@ -495,7 +531,9 @@
         vv=vmem((ALL, 1024), BF16),
         qq=vmem((ROWS, 512), BF16),
         gg=vmem((ROWS, 1024), BF16),
-        summ=vmem((NB + 1, 64, 1024), F32),
+        summ=vmem((NB, 64, 1024), F32),
+        kd=vmem((ROWS, 1024), BF16),
+        silu=vmem((ROWS, 1024), F32),
         ent=vmem((NB, 64, 1024), BF16),
         tots=vmem((8, 512), F32),
         ctx_msg=vmem((NTP, MSG, 128), BF16),
@@ -521,10 +559,8 @@
         up_w=vmem((32, 512), BF16),
         post_gain=vmem((1, D), F32),
         ready=vmem((ALL, D), F32),
-        result=vmem((ROWS, D), BF16),
         factor=vmem((ROWS, 128), F32),
         weight=vmem((8, D), F32),
-        out_sem=sems((4,)),
         load_sem=sems((17,)),
         m1s=sems((NSP - 1,)),
         m1r=sems((NSP - 1,)),
@@ -562,9 +598,9 @@
     hbm = pl.BlockSpec(memory_space=pl.ANY)
     return pl.pallas_call(
         kernel,
-        out_shape=jax.ShapeDtypeStruct((ROWS, D), BF16),
+        out_shape=pltpu.VMEM((ROWS, D), BF16),
         in_specs=[hbm] * 17,
-        out_specs=hbm,
+        out_specs=pl.BlockSpec(memory_space=pltpu.VMEM),
         scratch_shapes=[scratch()],
         compiler_params=pltpu.CompilerParams(
             collective_id=0, has_side_effects=True, vmem_limit_bytes=60 * 1024 * 1024

time: 45.4 us -> 41.7 us (0.919)
  Pallas kernels: 43 us -> 40.6 us
  local copies, waits for them, and re-layouts: 2.3 us -> 0.97 us
    pallas_call x1, Pallas kernels: 43 us -> 40.6 us  [shards(): pl.pallas_call(kernel, out_shape=pltpu.VMEM((ROWS, D), BF16), in_specs=[h...]
    unnamed x1, local copies, waits for them, and re-layouts: 2.3 us -> 0.97 us
where the time goes in v3:
time: 41.7 us; the launch traced here: 41.6 us
  Pallas kernels  40.6 us (97%)
  local copies, waits for them, and re-layouts  0.97 us (2%)
    pallas_call x1, Pallas kernels, shards(): pl.pallas_call(kernel, out_shape=pltpu.VMEM((ROWS, D), BF16), in_specs=[h...  40.6 us
    unnamed x1, local copies, waits for them, and re-layouts  0.97 us

profile of v3, /device:TPU:1, one launch (start us, length us, event | category | flops | bytes accessed | tf_op | source)
XLA Modules:
  0.0 41.6 jit_solution(16202662759260027307)
XLA Ops:
  0.0 40.6 %shard_map.163 = bf16[256,2048]{1,0:T(8,128)(2,1)S(1)} custom-call(bf16[256,2048]{1,0:T(8,128)(2,1)} %latent.1, bf16[32,2048]{1,0:T(8,128)(2,1)} %context.1, bf16[16,128]{1,0:T(8,128)(2,1)} %bitcast.9, bf16[16,128]{1,0:T(8,128)(2,1)} %bitcast.10, bf16[128,256]{1,0:T(8,128)(2,1)} %shift_w.1, bf16[128,256]{1,0:T(8,128)(2,1)} %scale_w.1, ...), custom_call_target="tpu_custom_call" | custom-call | tf_op jit(solution)/shard_map/pallas_call | solution.py:599
  40.6 1.0 %copy.19 = bf16[256,2048]{1,0:T(8,128)(2,1)} copy(bf16[256,2048]{1,0:T(8,128)(2,1)S(1)} %shard_map.163) | data formatting | bytes 2097152

commit v4 on v3

--- a/solution.py
+++ b/solution.py
@@ -153,7 +153,9 @@
 
     sends = []
 
-    def exchange(axis, src, dst, send_sem, recv_sem):
+    flip = lax.div(tp, NTP // 2)
+
+    def exchange(axis, src, dst, send_sem, recv_sem, ordered=False):
         steps, peer = (SP_STEPS, sp_peer) if axis == "sp" else (TP_STEPS, tp_peer)
         for d, step in enumerate(steps):
             to = peer(step)
@@ -165,23 +167,31 @@
                 device_id=(to, tp) if axis == "sp" else (sp, to),
                 device_id_type=MESH,
             )
-            copy.start()
-            sends.append(copy)
-
-    def arrive(axis, dst, send_sem, recv_sem):
+            later = (to - sp) * (1 - 2 * flip) > 0 if ordered else None
+            if ordered:
+                pl.when(later)(copy.start)
+            else:
+                copy.start()
+            sends.append((copy, later))
+
+    def arrive(axis, dst, send_sem, recv_sem, ordered=False):
         steps, wrap, peer = (
             (SP_STEPS, (4, 4), sp_peer) if axis == "sp" else (TP_STEPS, (4, 2), tp_peer)
         )
         for d, step in reversed(list(enumerate(steps))):
             origin = peer((wrap[0] - step[0], wrap[1] - step[1]))
-            pltpu.make_async_remote_copy(
+            copy = pltpu.make_async_remote_copy(
                 src_ref=dst(origin),
                 dst_ref=dst(origin),
                 send_sem=send_sem.at[d],
                 recv_sem=recv_sem.at[d],
                 device_id=(origin, tp) if axis == "sp" else (sp, origin),
                 device_id_type=MESH,
-            ).wait_recv()
+            )
+            if ordered:
+                pl.when((sp - origin) * (1 - 2 * flip) > 0)(copy.wait_recv)
+            else:
+                copy.wait_recv()
 
     loaded("lat_cond", "ctx_cond", "shift", "scale", "gate")
     row16 = iota((16, 128), 0)
@@ -267,8 +277,12 @@
             vv[rows, at] = dot(normed[rows, :], s["wv"][:, at]).astype(BF16)
 
     own, ctx_rows = slice(0, ROWS), slice(ROWS, ALL)
-    project(own)
+    low = dot_dims(normed[own, :], s["wd"][...], 1, 1).astype(BF16)
+    kk[own, :] = dot(normed[own, :], s["wk"][...]).astype(BF16)
+    ld[own, :] = log_decays(dot(low, s["up_w"][...]) + s["bias"][...])
+    vv[own, 0:512] = dot(normed[own, :], s["wv"][:, 0:512]).astype(BF16)
     lcum[own, :] = sum_rows(tri[...], ld[own, :])
+    vv[own, 512:1024] = dot(normed[own, :], s["wv"][:, 512:1024]).astype(BF16)
 
     ent, tots, kd = s["ent"], s["tots"], s["kd"]
     ctx_msg, seg_msg = s["ctx_msg"], s["seg_msg"]
@@ -369,7 +383,6 @@
                 ent[n, :, at] = run.astype(BF16)
                 run = close[n] * run + summ[n, :, at]
 
-    flip = lax.div(tp, NTP // 2)
     arrive("tp", lambda i: recv_a.at[i], s["as"], s["ar"])
     pre_s, pre_c = s["pre_s"], s["pre_c"]
     run = jnp.zeros((64, 128), F32)
@@ -382,7 +395,7 @@
         run = jnp.exp(total) * run + state
         run_log = run_log + total
     put_message(grp_all, sp, run, run_log)
-    exchange("sp", lambda to: grp_all.at[sp], lambda i: grp_all.at[i], s["gs"], s["gr"])
+    exchange("sp", lambda to: grp_all.at[sp], lambda i: grp_all.at[i], s["gs"], s["gr"], True)
 
 
     @pl.loop(0, 2)
@@ -445,7 +458,7 @@
     for i in range(NSP):
         state, total = get_message(ctx_all, i + flip * (NSP - 1 - 2 * i))
         reach = jnp.exp(total) * reach + state
-    arrive("sp", lambda i: grp_all.at[i], s["gs"], s["gr"])
+    arrive("sp", lambda i: grp_all.at[i], s["gs"], s["gr"], True)
     rank = sp + flip * (NSP - 1 - 2 * sp)
     for i in range(NSP):
         state, total = get_message(grp_all, i + flip * (NSP - 1 - 2 * i))
@@ -482,28 +495,29 @@
         gated[:, v_at] = (normal * silu[:, v_at]).astype(BF16)
 
     branch = s["branch"]
-    squares = jnp.zeros((ROWS, 128), F32)
-    for i in range(4):
-        at = slice(i * 512, (i + 1) * 512)
-        part = dot(gated[...], s["wo"][:, at]).astype(BF16)
-        branch[:, at] = part
-        part = part.astype(F32)
-        part = part * part
-        for j in range(4):
-            squares = squares + part[:, j * 128 : (j + 1) * 128]
-    mean = jnp.sum(squares, axis=-1, keepdims=True) * (1.0 / D)
-    s["factor"][...] = jnp.broadcast_to(lax.rsqrt(mean + EPS), (ROWS, 128))
-
-    @pl.loop(0, ROWS // 16)
-    def _(i):
-        at = pl.ds(pl.multiple_of(i * 16, 16), 16)
-        factor = s["factor"][at, 0:1]
-        added = branch[at, :].astype(F32) * factor * weight[0:1, :]
-        out[at, :] = (lat[at, :].astype(F32) + added).astype(BF16)
-
-
-    for copy in sends:
-        copy.wait_send()
+    for half in range(1):
+        rows = slice(half * 256, (half + 1) * 256)
+        squares = jnp.zeros((256, 128), F32)
+        for i in range(8):
+            at = slice(i * 256, (i + 1) * 256)
+            part = dot(gated[rows, :], s["wo"][:, at]).astype(BF16)
+            branch[rows, at] = part
+            part = part.astype(F32)
+            part = part * part
+            for j in range(2):
+                squares = squares + part[:, j * 128 : (j + 1) * 128]
+        mean = jnp.sum(squares, axis=-1, keepdims=True) * (1.0 / D)
+        factors = lax.rsqrt(mean + EPS)
+        for k in range(16):
+            at = slice(half * 256 + k * 16, half * 256 + (k + 1) * 16)
+            added = branch[at, :].astype(F32) * factors[k * 16 : (k + 1) * 16] * weight[0:1, :]
+            out[at, :] = (lat[at, :].astype(F32) + added).astype(BF16)
+
+    for copy, later in sends:
+        if later is None:
+            copy.wait_send()
+        else:
+            pl.when(later)(copy.wait_send)
 
 
 def scratch():

time: 41.7 us -> 39.5 us (0.947)
  Pallas kernels: 40.6 us -> 38.4 us
    pallas_call x1, Pallas kernels: 40.6 us -> 38.4 us  [shards(): pl.pallas_call(kernel, out_shape=pltpu.VMEM((ROWS, D), BF16), in_specs=[h...]
where the time goes in v4:
time: 39.5 us; the launch traced here: 39.4 us
  Pallas kernels  38.4 us (97%)
  local copies, waits for them, and re-layouts  0.97 us (2%)
    pallas_call x1, Pallas kernels, shards(): pl.pallas_call(kernel, out_shape=pltpu.VMEM((ROWS, D), BF16), in_specs=[h...  38.4 us
    unnamed x1, local copies, waits for them, and re-layouts  0.97 us

profile of v4, /device:TPU:1, one launch (start us, length us, event | category | flops | bytes accessed | tf_op | source)
XLA Modules:
  0.0 39.4 jit_solution(5246765370772073882)
XLA Ops:
  0.0 38.4 %shard_map.163 = bf16[256,2048]{1,0:T(8,128)(2,1)S(1)} custom-call(bf16[256,2048]{1,0:T(8,128)(2,1)} %latent.1, bf16[32,2048]{1,0:T(8,128)(2,1)} %context.1, bf16[16,128]{1,0:T(8,128)(2,1)} %bitcast.9, bf16[16,128]{1,0:T(8,128)(2,1)} %bitcast.10, bf16[128,256]{1,0:T(8,128)(2,1)} %shift_w.1, bf16[128,256]{1,0:T(8,128)(2,1)} %scale_w.1, ...), custom_call_target="tpu_custom_call" | custom-call | tf_op jit(solution)/shard_map/pallas_call | solution.py:613
  38.4 1.0 %copy.19 = bf16[256,2048]{1,0:T(8,128)(2,1)} copy(bf16[256,2048]{1,0:T(8,128)(2,1)S(1)} %shard_map.163) | data formatting | bytes 2097152

commit v5 on v4

--- a/solution.py
+++ b/solution.py
@@ -174,11 +174,13 @@
                 copy.start()
             sends.append((copy, later))
 
-    def arrive(axis, dst, send_sem, recv_sem, ordered=False):
+    def arrive(axis, dst, send_sem, recv_sem, ordered=False, only=None):
         steps, wrap, peer = (
             (SP_STEPS, (4, 4), sp_peer) if axis == "sp" else (TP_STEPS, (4, 2), tp_peer)
         )
         for d, step in reversed(list(enumerate(steps))):
+            if only is not None and step != only:
+                continue
             origin = peer((wrap[0] - step[0], wrap[1] - step[1]))
             copy = pltpu.make_async_remote_copy(
                 src_ref=dst(origin),
@@ -209,7 +211,8 @@
         jnp.where(row8 < 4, dot(act, s["scale_w"][...])[0:8], dot(act, s["gate_w"][...])[0:8]),
     )
     mod1, mod2 = s["mod1"], s["mod2"]
-    mod1[sp] = part
+    mod1[sp, 0:5, :] = part[0:5, 0:128]
+    mod1[sp, 5:10, :] = part[0:5, 128:256]
     pl.semaphore_wait(barrier, NSP + NTP - 2)
     exchange("sp", lambda to: mod1.at[sp], lambda i: mod1.at[i], s["m1s"], s["m1r"])
 
@@ -249,40 +252,84 @@
         total = total + mod1[i]
     mod2[tp] = total
     exchange("tp", lambda to: mod2.at[tp], lambda i: mod2.at[i], s["m2s"], s["m2r"])
-    arrive("tp", lambda i: mod2.at[i], s["m2s"], s["m2r"])
-    modv = s["modv"]
-    for j in range(NTP):
-        modv[:, j * 256 : (j + 1) * 256] = mod2[j]
-
+    ld, lcum, kk, vv = s["ld"], s["lcum"], s["kk"], s["vv"]
+    acc, acc_low = s["acc"], s["acc_low"]
+    own, ctx_rows = slice(0, ROWS), slice(ROWS, ALL)
     loaded("bias", "up", "post", "down", "key", "value", "query", "outgate", "out")
 
-    def modulated(at, row):
-        scaled = ready[at, :] * (1.0 + modv[2 + row : 3 + row, :])
-        normed[at, :] = (scaled + modv[row : row + 1, :]).astype(BF16)
-
-    @pl.loop(0, ROWS // 32)
-    def _(i):
-        modulated(pl.ds(pl.multiple_of(i * 32, 32), 32), 0)
-
-    modulated(pl.ds(ROWS, CROWS), 1)
-
-    ld, lcum, kk, vv = s["ld"], s["lcum"], s["kk"], s["vv"]
+    def columns(origin):
+        return pl.ds(pl.multiple_of(origin * 256, 256), 256)
+
+    def modulate(origin):
+        slot = mod2[origin]
+
+        def row(i):
+            return jnp.concatenate([slot[i : i + 1], slot[5 + i : 6 + i]], axis=1)
+
+        cols = columns(origin)
+        for rows, i in ((own, 0), (ctx_rows, 1)):
+            values = ready[rows, cols] * (1.0 + row(2 + i)) + row(i)
+            normed[rows, cols] = values.astype(BF16)
+
+    def low_part(origin):
+        cols = columns(origin)
+        return dot_dims(normed[own, cols], s["wd"][:, cols], 1, 1)
+
+    def key_part(origin):
+        cols = columns(origin)
+        return dot(normed[own, cols], s["wk"][cols, :])
+
+    def value_part(origin, at):
+        cols = columns(origin)
+        return dot(normed[own, cols], s["wv"][cols, at])
+
+    v_half = (slice(0, 512), slice(512, 1024))
+    a_half = (slice(512, 1024), slice(1024, 1536))
+
+    def take(origin, first=False):
+        modulate(origin)
+        low, key = low_part(origin), key_part(origin)
+        acc_low[...] = low if first else acc_low[...] + low
+        acc[:, 0:512] = key if first else acc[:, 0:512] + key
+        for v_at, a_at in zip(v_half, a_half):
+            value = value_part(origin, v_at)
+            acc[:, a_at] = value if first else acc[:, a_at] + value
+
+    def tp_origin(step):
+        return tp_peer((4 - step[0], 2 - step[1]))
+
+    def arrive_mod(step):
+        arrive("tp", lambda i: mod2.at[i], s["m2s"], s["m2r"], only=step)
+
+    take(tp, True)
+    for step in ((0, 1), (1, 0), (3, 0), (1, 1), (3, 1)):
+        arrive_mod(step)
+        take(tp_origin(step))
+    last = ((2, 0), (2, 1))
+    for step in last:
+        arrive_mod(step)
+    one, two = (tp_origin(step) for step in last)
+    modulate(one)
+    modulate(two)
+    low = (acc_low[...] + low_part(one) + low_part(two)).astype(BF16)
+    kk[own, :] = (acc[:, 0:512] + key_part(one) + key_part(two)).astype(BF16)
+    ld[own, :] = log_decays(dot(low, s["up_w"][...]) + s["bias"][...])
+
+    def put_values(i):
+        at = v_half[i]
+        total = acc[:, a_half[i]] + value_part(one, at) + value_part(two, at)
+        vv[own, at] = total.astype(BF16)
+
+    put_values(0)
+    lcum[own, :] = sum_rows(tri[...], ld[own, :])
+    put_values(1)
 
     def project(rows):
         low = dot_dims(normed[rows, :], s["wd"][...], 1, 1).astype(BF16)
         ld[rows, :] = log_decays(dot(low, s["up_w"][...]) + s["bias"][...])
         kk[rows, :] = dot(normed[rows, :], s["wk"][...]).astype(BF16)
-        for i in range(2):
-            at = slice(i * 512, (i + 1) * 512)
+        for at in v_half:
             vv[rows, at] = dot(normed[rows, :], s["wv"][:, at]).astype(BF16)
-
-    own, ctx_rows = slice(0, ROWS), slice(ROWS, ALL)
-    low = dot_dims(normed[own, :], s["wd"][...], 1, 1).astype(BF16)
-    kk[own, :] = dot(normed[own, :], s["wk"][...]).astype(BF16)
-    ld[own, :] = log_decays(dot(low, s["up_w"][...]) + s["bias"][...])
-    vv[own, 0:512] = dot(normed[own, :], s["wv"][:, 0:512]).astype(BF16)
-    lcum[own, :] = sum_rows(tri[...], ld[own, :])
-    vv[own, 512:1024] = dot(normed[own, :], s["wv"][:, 512:1024]).astype(BF16)
 
     ent, tots, kd = s["ent"], s["tots"], s["kd"]
     ctx_msg, seg_msg = s["ctx_msg"], s["seg_msg"]
@@ -477,7 +524,10 @@
         silu[at, :] = gate * lax.logistic(gate)
 
     weight = s["weight"]
-    weight[...] = jnp.broadcast_to(modv[4:5, :] * s["post_gain"][...], (8, D))
+    for j in range(2 * NTP):
+        at = slice(j * 128, (j + 1) * 128)
+        gate_row = mod2[j // 2][4 + 5 * (j % 2) : 5 + 5 * (j % 2)]
+        weight[:, at] = jnp.broadcast_to(gate_row * s["post_gain"][:, at], (8, 128))
     arrive("tp", lambda i: recv_c.at[i], s["bs"], s["br"])
 
     gated = s["gated"]
@@ -531,9 +581,10 @@
         wq=vmem((D, 512), BF16),
         wg=vmem((D, 1024), BF16),
         wo=vmem((1024, D), BF16),
-        mod1=vmem((NSP, 8, 256), F32),
-        mod2=vmem((NTP, 8, 256), F32),
-        modv=vmem((8, D), F32),
+        mod1=vmem((NSP, 10, 128), F32),
+        mod2=vmem((NTP, 10, 128), F32),
+        acc=vmem((ROWS, 1536), F32),
+        acc_low=vmem((ROWS, 32), F32),
         normed=vmem((ALL, D), BF16),
         head128=vmem((256, 128), BF16),
         head256=vmem((256, 256), BF16),

time: 39.5 us -> 38.2 us (0.967)
  Pallas kernels: 38.4 us -> 37.1 us
    pallas_call x1, Pallas kernels: 38.4 us -> 37.1 us  [shards(): pl.pallas_call(kernel, out_shape=pltpu.VMEM((ROWS, D), BF16), in_specs=[h...]
where the time goes in v5:
time: 38.2 us; the launch traced here: 38.1 us
  Pallas kernels  37.1 us (97%)
  local copies, waits for them, and re-layouts  0.97 us (3%)
    pallas_call x1, Pallas kernels, shards(): pl.pallas_call(kernel, out_shape=pltpu.VMEM((ROWS, D), BF16), in_specs=[h...  37.1 us
    unnamed x1, local copies, waits for them, and re-layouts  0.97 us

profile of v5, /device:TPU:1, one launch (start us, length us, event | category | flops | bytes accessed | tf_op | source)
XLA Modules:
  0.0 38.1 jit_solution(17973604636621403344)
XLA Ops:
  0.0 37.1 %shard_map.163 = bf16[256,2048]{1,0:T(8,128)(2,1)S(1)} custom-call(bf16[256,2048]{1,0:T(8,128)(2,1)} %latent.1, bf16[32,2048]{1,0:T(8,128)(2,1)} %context.1, bf16[16,128]{1,0:T(8,128)(2,1)} %bitcast.9, bf16[16,128]{1,0:T(8,128)(2,1)} %bitcast.10, bf16[128,256]{1,0:T(8,128)(2,1)} %shift_w.1, bf16[128,256]{1,0:T(8,128)(2,1)} %scale_w.1, ...), custom_call_target="tpu_custom_call" | custom-call | tf_op jit(solution)/shard_map/pallas_call | solution.py:664
  37.1 1.0 %copy.19 = bf16[256,2048]{1,0:T(8,128)(2,1)} copy(bf16[256,2048]{1,0:T(8,128)(2,1)S(1)} %shard_map.163) | data formatting | bytes 2097152

commit v6 on v5

--- a/solution.py
+++ b/solution.py
@@ -153,7 +153,7 @@
 
     sends = []
 
-    flip = lax.div(tp, NTP // 2)
+    flip = c
 
     def exchange(axis, src, dst, send_sem, recv_sem, ordered=False):
         steps, peer = (SP_STEPS, sp_peer) if axis == "sp" else (TP_STEPS, tp_peer)
@@ -373,7 +373,7 @@
         for d in range(2):
             put_message(
                 seg_msg,
-                d * NG + g,
+                2 * g + d,
                 state[:, d * 128 : (d + 1) * 128],
                 whole[:, g * 128 : (g + 1) * 128],
             )
@@ -402,7 +402,7 @@
         for d in range(2):
             put_message(
                 ctx_msg,
-                d * NG + g,
+                2 * g + d,
                 state[:, d * 128 : (d + 1) * 128],
                 ctx_total[:, g * 128 : (g + 1) * 128],
             )
@@ -528,13 +528,17 @@
         at = slice(j * 128, (j + 1) * 128)
         gate_row = mod2[j // 2][4 + 5 * (j % 2) : 5 + 5 * (j % 2)]
         weight[:, at] = jnp.broadcast_to(gate_row * s["post_gain"][:, at], (8, 128))
-    arrive("tp", lambda i: recv_c.at[i], s["bs"], s["br"])
-
-    gated = s["gated"]
-    for g in range(NG):
-        v_at = slice(g * 256, (g + 1) * 256)
+
+    acc_out = s["acc_out"]
+
+    def gated_group(dy):
+        for dc in (0, 1):
+            if (dy, dc) != (0, 0):
+                arrive("tp", lambda i: recv_c.at[i], s["bs"], s["br"], only=(dy, dc))
+        g = lax.rem(y + 4 - dy, 4)
+        v_at = pl.ds(pl.multiple_of(g * 256, 256), 256)
         states = jnp.concatenate(
-            [four(recv_c[g], head128[...]), four(recv_c[NG + g], head128[...])], axis=1
+            [four(recv_c[2 * g], head128[...]), four(recv_c[2 * g + 1], head128[...])], axis=1
         )
         values = mixed[:, v_at] + dot_dims(qd[:, v_at], states, 1, 1)
         square = values * values
@@ -542,26 +546,32 @@
         low = (square - hi.astype(F32)).astype(BF16)
         power = dot(hi, ones[...]) + dot(low, ones[...])
         normal = values * lax.rsqrt(power * (1.0 / DV) + EPS)
-        gated[:, v_at] = (normal * silu[:, v_at]).astype(BF16)
+        return (normal * silu[:, v_at]).astype(BF16), v_at
+
+    for i, dy in enumerate((0, 1, 3)):
+        gated, k_rows = gated_group(dy)
+        for j in range(4):
+            at = slice(j * 512, (j + 1) * 512)
+            part = dot(gated, s["wo"][k_rows, at])
+            acc_out[:, at] = part if i == 0 else acc_out[:, at] + part
+    gated, k_rows = gated_group(2)
 
     branch = s["branch"]
-    for half in range(1):
-        rows = slice(half * 256, (half + 1) * 256)
-        squares = jnp.zeros((256, 128), F32)
-        for i in range(8):
-            at = slice(i * 256, (i + 1) * 256)
-            part = dot(gated[rows, :], s["wo"][:, at]).astype(BF16)
-            branch[rows, at] = part
-            part = part.astype(F32)
-            part = part * part
-            for j in range(2):
-                squares = squares + part[:, j * 128 : (j + 1) * 128]
-        mean = jnp.sum(squares, axis=-1, keepdims=True) * (1.0 / D)
-        factors = lax.rsqrt(mean + EPS)
-        for k in range(16):
-            at = slice(half * 256 + k * 16, half * 256 + (k + 1) * 16)
-            added = branch[at, :].astype(F32) * factors[k * 16 : (k + 1) * 16] * weight[0:1, :]
-            out[at, :] = (lat[at, :].astype(F32) + added).astype(BF16)
+    squares = jnp.zeros((ROWS, 128), F32)
+    for i in range(8):
+        at = slice(i * 256, (i + 1) * 256)
+        part = (acc_out[:, at] + dot(gated, s["wo"][k_rows, at])).astype(BF16)
+        branch[:, at] = part
+        part = part.astype(F32)
+        part = part * part
+        for j in range(2):
+            squares = squares + part[:, j * 128 : (j + 1) * 128]
+    mean = jnp.sum(squares, axis=-1, keepdims=True) * (1.0 / D)
+    factors = lax.rsqrt(mean + EPS)
+    for k in range(ROWS // 16):
+        at = slice(k * 16, (k + 1) * 16)
+        added = branch[at, :].astype(F32) * factors[at] * weight[0:1, :]
+        out[at, :] = (lat[at, :].astype(F32) + added).astype(BF16)
 
     for copy, later in sends:
         if later is None:
@@ -612,7 +622,7 @@
         recv_c=vmem((NTP, 64, 128), BF16),
         mixed=vmem((ROWS, 1024), F32),
         qd=vmem((ROWS, 1024), BF16),
-        gated=vmem((ROWS, 1024), BF16),
+        acc_out=vmem((ROWS, D), F32),
         branch=vmem((ROWS, D), BF16),
         lat_cond=vmem((16, 128), BF16),
         ctx_cond=vmem((16, 128), BF16),
@@ -624,7 +634,6 @@
         up_w=vmem((32, 512), BF16),
         post_gain=vmem((1, D), F32),
         ready=vmem((ALL, D), F32),
-        factor=vmem((ROWS, 128), F32),
         weight=vmem((8, D), F32),
         load_sem=sems((17,)),
         m1s=sems((NSP - 1,)),

time: 38.2 us -> 36.6 us (0.958)
  Pallas kernels: 37.1 us -> 35.5 us
    pallas_call x1, Pallas kernels: 37.1 us -> 35.5 us  [shards(): pl.pallas_call(kernel, out_shape=pltpu.VMEM((ROWS, D), BF16), in_specs=[h...]
where the time goes in v6:
time: 36.6 us; the launch traced here: 36.5 us
  Pallas kernels  35.5 us (97%)
  local copies, waits for them, and re-layouts  0.97 us (3%)
    pallas_call x1, Pallas kernels, shards(): pl.pallas_call(kernel, out_shape=pltpu.VMEM((ROWS, D), BF16), in_specs=[h...  35.5 us
    unnamed x1, local copies, waits for them, and re-layouts  0.97 us

profile of v6, /device:TPU:1, one launch (start us, length us, event | category | flops | bytes accessed | tf_op | source)
XLA Modules:
  0.0 36.5 jit_solution(2436828695282414849)
XLA Ops:
  0.0 35.5 %shard_map.163 = bf16[256,2048]{1,0:T(8,128)(2,1)S(1)} custom-call(bf16[256,2048]{1,0:T(8,128)(2,1)} %latent.1, bf16[32,2048]{1,0:T(8,128)(2,1)} %context.1, bf16[16,128]{1,0:T(8,128)(2,1)} %bitcast.9, bf16[16,128]{1,0:T(8,128)(2,1)} %bitcast.10, bf16[128,256]{1,0:T(8,128)(2,1)} %shift_w.1, bf16[128,256]{1,0:T(8,128)(2,1)} %scale_w.1, ...), custom_call_target="tpu_custom_call" | custom-call | tf_op jit(solution)/shard_map/pallas_call | solution.py:673
  35.5 1.0 %copy.19 = bf16[256,2048]{1,0:T(8,128)(2,1)} copy(bf16[256,2048]{1,0:T(8,128)(2,1)S(1)} %shard_map.163) | data formatting | bytes 2097152

commit v7 on v6

--- a/solution.py
+++ b/solution.py
@@ -155,9 +155,11 @@
 
     flip = c
 
-    def exchange(axis, src, dst, send_sem, recv_sem, ordered=False):
+    def exchange(axis, src, dst, send_sem, recv_sem, ordered=False, only=None):
         steps, peer = (SP_STEPS, sp_peer) if axis == "sp" else (TP_STEPS, tp_peer)
         for d, step in enumerate(steps):
+            if only is not None and step[0] != only:
+                continue
             to = peer(step)
             copy = pltpu.make_async_remote_copy(
                 src_ref=src(to),
@@ -367,18 +369,18 @@
             kd[rows, g * 256 : (g + 1) * 256] = jnp.concatenate(
                 [key_f[:, k_at], key_b[:, k_at]], axis=1
             )
-    for g in range(NG):
-        v_at = slice(g * 256, (g + 1) * 256)
+    tots[NB : NB + 1, :] = whole
+    for dy in (2, 1, 3, 0):
+        g = lax.rem(y + dy, 4)
+        v_at = pl.ds(pl.multiple_of(g * 256, 256), 256)
         state = own_lanes(dot_dims(vv[own, v_at], kd[:, v_at], 0, 0))
+        whole_g = tots[NB : NB + 1, pl.ds(pl.multiple_of(g * 128, 128), 128)]
         for d in range(2):
-            put_message(
-                seg_msg,
-                2 * g + d,
-                state[:, d * 128 : (d + 1) * 128],
-                whole[:, g * 128 : (g + 1) * 128],
-            )
+            put_message(seg_msg, 2 * g + d, state[:, d * 128 : (d + 1) * 128], whole_g)
+        exchange(
+            "tp", lambda to: seg_msg.at[to], lambda i: recv_a.at[i], s["as"], s["ar"], only=dy
+        )
     recv_a[tp] = seg_msg[tp]
-    exchange("tp", lambda to: seg_msg.at[to], lambda i: recv_a.at[i], s["as"], s["ar"])
 
     project(ctx_rows)
     lcum[ctx_rows, :] = sum_rows(tri[0:CROWS, 0:CROWS], ld[ctx_rows, :])
@@ -510,10 +512,14 @@
     for i in range(NSP):
         state, total = get_message(grp_all, i + flip * (NSP - 1 - 2 * i))
         reach = jnp.where(i < rank, jnp.exp(total) * reach + state, reach)
-    for j in range(NTP):
-        back[j] = (pre_s[j] + jnp.exp(pre_c[j][0:1]) * reach).astype(BF16)
+    for dy in (2, 1, 3, 0):
+        for dc in range(2):
+            j = tp_peer((dy, dc))
+            back[j] = (pre_s[j] + jnp.exp(pre_c[j][0:1]) * reach).astype(BF16)
+        exchange(
+            "tp", lambda to: back.at[to], lambda i: recv_c.at[i], s["bs"], s["br"], only=dy
+        )
     recv_c[tp] = back[tp]
-    exchange("tp", lambda to: back.at[to], lambda i: recv_c.at[i], s["bs"], s["br"])
     ones[...] = head256[...]
     silu = s["silu"]
 

time: 36.6 us -> 37 us (1.011)
  Pallas kernels: 35.5 us -> 35.9 us
    pallas_call x1, Pallas kernels: 35.5 us -> 35.9 us  [shards(): pl.pallas_call(kernel, out_shape=pltpu.VMEM((ROWS, D), BF16), in_specs=[h...]
where the time goes in v7:
time: 37 us; the launch traced here: 36.8 us
  Pallas kernels  35.9 us (97%)
  local copies, waits for them, and re-layouts  0.97 us (3%)
    pallas_call x1, Pallas kernels, shards(): pl.pallas_call(kernel, out_shape=pltpu.VMEM((ROWS, D), BF16), in_specs=[h...  35.9 us
    unnamed x1, local copies, waits for them, and re-layouts  0.97 us

profile of v7, /device:TPU:1, one launch (start us, length us, event | category | flops | bytes accessed | tf_op | source)
XLA Modules:
  0.0 36.8 jit_solution(17753727052646170395)
XLA Ops:
  0.0 35.9 %shard_map.163 = bf16[256,2048]{1,0:T(8,128)(2,1)S(1)} custom-call(bf16[256,2048]{1,0:T(8,128)(2,1)} %latent.1, bf16[32,2048]{1,0:T(8,128)(2,1)} %context.1, bf16[16,128]{1,0:T(8,128)(2,1)} %bitcast.9, bf16[16,128]{1,0:T(8,128)(2,1)} %bitcast.10, bf16[128,256]{1,0:T(8,128)(2,1)} %shift_w.1, bf16[128,256]{1,0:T(8,128)(2,1)} %scale_w.1, ...), custom_call_target="tpu_custom_call" | custom-call | tf_op jit(solution)/shard_map/pallas_call | solution.py:679
  35.9 1.0 %copy.19 = bf16[256,2048]{1,0:T(8,128)(2,1)} copy(bf16[256,2048]{1,0:T(8,128)(2,1)S(1)} %shard_map.163) | data formatting | bytes 2097152

commit v8 on v6

--- a/solution.py
+++ b/solution.py
@@ -204,15 +204,16 @@
 
     cond = jnp.where(lax.rem(row16, 2) == 0, cond_row("lat_cond"), cond_row("ctx_cond"))
     act = (cond * lax.logistic(cond)).astype(BF16)
-    row8 = iota((8, 256), 0)
-    part = jnp.where(
-        row8 < 2,
-        dot(act, s["shift_w"][...])[0:8],
-        jnp.where(row8 < 4, dot(act, s["scale_w"][...])[0:8], dot(act, s["gate_w"][...])[0:8]),
+    shift_part, scale_part, gate_part = (
+        dot(act, s[name][...])[0:8] for name in ("shift_w", "scale_w", "gate_w")
     )
+    gate1, gate2 = s["gate1"], s["gate2"]
+    for i in range(2):
+        half = slice(i * 128, (i + 1) * 128)
+        s["mod1"][sp, 4 * i : 4 * i + 2, :] = shift_part[0:2, half]
+        s["mod1"][sp, 4 * i + 2 : 4 * i + 4, :] = scale_part[0:2, half]
+        gate1[sp, i : i + 1, :] = gate_part[0:1, half]
     mod1, mod2 = s["mod1"], s["mod2"]
-    mod1[sp, 0:5, :] = part[0:5, 0:128]
-    mod1[sp, 5:10, :] = part[0:5, 128:256]
     pl.semaphore_wait(barrier, NSP + NTP - 2)
     exchange("sp", lambda to: mod1.at[sp], lambda i: mod1.at[i], s["m1s"], s["m1r"])
 
@@ -252,6 +253,7 @@
         total = total + mod1[i]
     mod2[tp] = total
     exchange("tp", lambda to: mod2.at[tp], lambda i: mod2.at[i], s["m2s"], s["m2r"])
+    exchange("sp", lambda to: gate1.at[sp], lambda i: gate1.at[i], s["g1s"], s["g1r"])
     ld, lcum, kk, vv = s["ld"], s["lcum"], s["kk"], s["vv"]
     acc, acc_low = s["acc"], s["acc_low"]
     own, ctx_rows = slice(0, ROWS), slice(ROWS, ALL)
@@ -264,7 +266,7 @@
         slot = mod2[origin]
 
         def row(i):
-            return jnp.concatenate([slot[i : i + 1], slot[5 + i : 6 + i]], axis=1)
+            return jnp.concatenate([slot[i : i + 1], slot[4 + i : 5 + i]], axis=1)
 
         cols = columns(origin)
         for rows, i in ((own, 0), (ctx_rows, 1)):
@@ -429,6 +431,13 @@
             for n in range(NB) if d == 0 else reversed(range(NB)):
                 ent[n, :, at] = run.astype(BF16)
                 run = close[n] * run + summ[n, :, at]
+
+    arrive("sp", lambda i: gate1.at[i], s["g1s"], s["g1r"])
+    total = gate1[0]
+    for i in range(1, NSP):
+        total = total + gate1[i]
+    gate2[tp] = total
+    exchange("tp", lambda to: gate2.at[tp], lambda i: gate2.at[i], s["g2s"], s["g2r"])
 
     arrive("tp", lambda i: recv_a.at[i], s["as"], s["ar"])
     pre_s, pre_c = s["pre_s"], s["pre_c"]
@@ -524,9 +533,10 @@
         silu[at, :] = gate * lax.logistic(gate)
 
     weight = s["weight"]
+    arrive("tp", lambda i: gate2.at[i], s["g2s"], s["g2r"])
     for j in range(2 * NTP):
         at = slice(j * 128, (j + 1) * 128)
-        gate_row = mod2[j // 2][4 + 5 * (j % 2) : 5 + 5 * (j % 2)]
+        gate_row = gate2[j // 2][j % 2 : j % 2 + 1]
         weight[:, at] = jnp.broadcast_to(gate_row * s["post_gain"][:, at], (8, 128))
 
     acc_out = s["acc_out"]
@@ -591,8 +601,10 @@
         wq=vmem((D, 512), BF16),
         wg=vmem((D, 1024), BF16),
         wo=vmem((1024, D), BF16),
-        mod1=vmem((NSP, 10, 128), F32),
-        mod2=vmem((NTP, 10, 128), F32),
+        mod1=vmem((NSP, 8, 128), F32),
+        gate1=vmem((NSP, 2, 128), F32),
+        mod2=vmem((NTP, 8, 128), F32),
+        gate2=vmem((NTP, 2, 128), F32),
         acc=vmem((ROWS, 1536), F32),
         acc_low=vmem((ROWS, 32), F32),
         normed=vmem((ALL, D), BF16),
@@ -636,6 +648,10 @@
         ready=vmem((ALL, D), F32),
         weight=vmem((8, D), F32),
         load_sem=sems((17,)),
+        g1s=sems((NSP - 1,)),
+        g1r=sems((NSP - 1,)),
+        g2s=sems((NTP - 1,)),
+        g2r=sems((NTP - 1,)),
         m1s=sems((NSP - 1,)),
         m1r=sems((NSP - 1,)),
         m2s=sems((NTP - 1,)),

time: 36.6 us -> 36.9 us (level)
  no operation moved by 1% of the time
where the time goes in v8:
time: 36.9 us; the launch traced here: 36.8 us
  Pallas kernels  35.8 us (97%)
  local copies, waits for them, and re-layouts  0.97 us (3%)
    pallas_call x1, Pallas kernels, shards(): pl.pallas_call(kernel, out_shape=pltpu.VMEM((ROWS, D), BF16), in_specs=[h...  35.8 us
    unnamed x1, local copies, waits for them, and re-layouts  0.97 us

profile of v8, /device:TPU:1, one launch (start us, length us, event | category | flops | bytes accessed | tf_op | source)
XLA Modules:
  0.0 36.8 jit_solution(10502862308051467529)
XLA Ops:
  0.0 35.8 %shard_map.163 = bf16[256,2048]{1,0:T(8,128)(2,1)S(1)} custom-call(bf16[256,2048]{1,0:T(8,128)(2,1)} %latent.1, bf16[32,2048]{1,0:T(8,128)(2,1)} %context.1, bf16[16,128]{1,0:T(8,128)(2,1)} %bitcast.9, bf16[16,128]{1,0:T(8,128)(2,1)} %bitcast.10, bf16[128,256]{1,0:T(8,128)(2,1)} %shift_w.1, bf16[128,256]{1,0:T(8,128)(2,1)} %scale_w.1, ...), custom_call_target="tpu_custom_call" | custom-call | tf_op jit(solution)/shard_map/pallas_call | solution.py:689
  35.8 1.0 %copy.19 = bf16[256,2048]{1,0:T(8,128)(2,1)} copy(bf16[256,2048]{1,0:T(8,128)(2,1)S(1)} %shard_map.163) | data formatting | bytes 2097152

commit v9 on v6

--- a/solution.py
+++ b/solution.py
@@ -151,28 +151,33 @@
         for name in names:
             loads[name].wait()
 
-    sends = []
+    sends, bulk = [], []
 
     flip = c
 
-    def exchange(axis, src, dst, send_sem, recv_sem, ordered=False):
+    def exchange(axis, src, dst, send_sem, recv_sem, slots=None, once=False):
         steps, peer = (SP_STEPS, sp_peer) if axis == "sp" else (TP_STEPS, tp_peer)
         for d, step in enumerate(steps):
             to = peer(step)
             copy = pltpu.make_async_remote_copy(
                 src_ref=src(to),
                 dst_ref=dst(sp if axis == "sp" else tp),
-                send_sem=send_sem.at[d],
-                recv_sem=recv_sem.at[d],
+                send_sem=send_sem.at[0 if slots is not None else d],
+                recv_sem=recv_sem.at[0 if once else d],
                 device_id=(to, tp) if axis == "sp" else (sp, to),
                 device_id_type=MESH,
             )
-            later = (to - sp) * (1 - 2 * flip) > 0 if ordered else None
-            if ordered:
+            if slots is None:
+                later = (to - sp) * (1 - 2 * flip) > 0
                 pl.when(later)(copy.start)
+                sends.append((copy, later))
             else:
                 copy.start()
-            sends.append((copy, later))
+        if slots is not None:
+            bulk.append((slots.at[pl.ds(0, len(steps))], send_sem.at[0]))
+
+    def wait_bulk(slots, sem):
+        pltpu.make_async_copy(slots, slots, sem).wait()
 
     def arrive(axis, dst, send_sem, recv_sem, ordered=False, only=None):
         steps, wrap, peer = (
@@ -185,7 +190,7 @@
             copy = pltpu.make_async_remote_copy(
                 src_ref=dst(origin),
                 dst_ref=dst(origin),
-                send_sem=send_sem.at[d],
+                send_sem=send_sem.at[d if ordered else 0],
                 recv_sem=recv_sem.at[d],
                 device_id=(origin, tp) if axis == "sp" else (sp, origin),
                 device_id_type=MESH,
@@ -214,7 +219,7 @@
     mod1[sp, 0:5, :] = part[0:5, 0:128]
     mod1[sp, 5:10, :] = part[0:5, 128:256]
     pl.semaphore_wait(barrier, NSP + NTP - 2)
-    exchange("sp", lambda to: mod1.at[sp], lambda i: mod1.at[i], s["m1s"], s["m1r"])
+    exchange("sp", lambda to: mod1.at[sp], lambda i: mod1.at[i], s["m1s"], s["m1r"], mod1, True)
 
     head128, head256, tri, ones = s["head128"], s["head256"], s["tri"], s["ones"]
 
@@ -246,12 +251,12 @@
         at = pl.ds(pl.multiple_of(i * 16, 16), 16)
         ready[at, :] = norm_rows(lat[at, :])
 
-    arrive("sp", lambda i: mod1.at[i], s["m1s"], s["m1r"])
+    wait_bulk(mod1.at[pl.ds(0, NSP - 1)], s["m1r"].at[0])
     total = mod1[0]
     for i in range(1, NSP):
         total = total + mod1[i]
     mod2[tp] = total
-    exchange("tp", lambda to: mod2.at[tp], lambda i: mod2.at[i], s["m2s"], s["m2r"])
+    exchange("tp", lambda to: mod2.at[tp], lambda i: mod2.at[i], s["m2s"], s["m2r"], mod2)
     ld, lcum, kk, vv = s["ld"], s["lcum"], s["kk"], s["vv"]
     acc, acc_low = s["acc"], s["acc_low"]
     own, ctx_rows = slice(0, ROWS), slice(ROWS, ALL)
@@ -378,7 +383,7 @@
                 whole[:, g * 128 : (g + 1) * 128],
             )
     recv_a[tp] = seg_msg[tp]
-    exchange("tp", lambda to: seg_msg.at[to], lambda i: recv_a.at[i], s["as"], s["ar"])
+    exchange("tp", lambda to: seg_msg.at[to], lambda i: recv_a.at[i], s["as"], s["ar"], recv_a, True)
 
     project(ctx_rows)
     lcum[ctx_rows, :] = sum_rows(tri[0:CROWS, 0:CROWS], ld[ctx_rows, :])
@@ -409,7 +414,7 @@
 
     summaries(ctx_rows, CROWS, put_context)
     ctx_all[sp] = ctx_msg[tp]
-    exchange("sp", lambda to: ctx_all.at[sp], lambda i: ctx_all.at[i], s["cs"], s["cr"])
+    exchange("sp", lambda to: ctx_all.at[sp], lambda i: ctx_all.at[i], s["cs"], s["cr"], ctx_all, True)
 
     qq, gg = s["qq"], s["gg"]
     qq[...] = dot(normed[0:ROWS, :], s["wq"][...]).astype(BF16)
@@ -430,7 +435,7 @@
                 ent[n, :, at] = run.astype(BF16)
                 run = close[n] * run + summ[n, :, at]
 
-    arrive("tp", lambda i: recv_a.at[i], s["as"], s["ar"])
+    wait_bulk(recv_a.at[pl.ds(0, NTP - 1)], s["ar"].at[0])
     pre_s, pre_c = s["pre_s"], s["pre_c"]
     run = jnp.zeros((64, 128), F32)
     run_log = jnp.zeros((1, 128), F32)
@@ -442,7 +447,7 @@
         run = jnp.exp(total) * run + state
         run_log = run_log + total
     put_message(grp_all, sp, run, run_log)
-    exchange("sp", lambda to: grp_all.at[sp], lambda i: grp_all.at[i], s["gs"], s["gr"], True)
+    exchange("sp", lambda to: grp_all.at[sp], lambda i: grp_all.at[i], s["gs"], s["gr"])
 
 
     @pl.loop(0, 2)
@@ -500,7 +505,7 @@
             )
             mixed[rows, v_at] = within + across
 
-    arrive("sp", lambda i: ctx_all.at[i], s["cs"], s["cr"])
+    wait_bulk(ctx_all.at[pl.ds(0, NSP - 1)], s["cr"].at[0])
     reach = jnp.zeros((64, 128), F32)
     for i in range(NSP):
         state, total = get_message(ctx_all, i + flip * (NSP - 1 - 2 * i))
@@ -513,7 +518,7 @@
     for j in range(NTP):
         back[j] = (pre_s[j] + jnp.exp(pre_c[j][0:1]) * reach).astype(BF16)
     recv_c[tp] = back[tp]
-    exchange("tp", lambda to: back.at[to], lambda i: recv_c.at[i], s["bs"], s["br"])
+    exchange("tp", lambda to: back.at[to], lambda i: recv_c.at[i], s["bs"], s["br"], recv_c)
     ones[...] = head256[...]
     silu = s["silu"]
 
@@ -574,10 +579,9 @@
         out[at, :] = (lat[at, :].astype(F32) + added).astype(BF16)
 
     for copy, later in sends:
-        if later is None:
-            copy.wait_send()
-        else:
-            pl.when(later)(copy.wait_send)
+        pl.when(later)(copy.wait_send)
+    for slots, sem in bulk:
+        wait_bulk(slots, sem)
 
 
 def scratch():
@@ -636,17 +640,17 @@
         ready=vmem((ALL, D), F32),
         weight=vmem((8, D), F32),
         load_sem=sems((17,)),
-        m1s=sems((NSP - 1,)),
-        m1r=sems((NSP - 1,)),
-        m2s=sems((NTP - 1,)),
+        m1s=sems((1,)),
+        m1r=sems((1,)),
+        m2s=sems((1,)),
         m2r=sems((NTP - 1,)),
-        cs=sems((NSP - 1,)),
-        cr=sems((NSP - 1,)),
+        cs=sems((1,)),
+        cr=sems((1,)),
         gs=sems((NSP - 1,)),
         gr=sems((NSP - 1,)),
-        bs=sems((NTP - 1,)),
+        bs=sems((1,)),
         br=sems((NTP - 1,)),
-        **{"as": sems((NTP - 1,)), "ar": sems((NTP - 1,))},
+        **{"as": sems((1,)), "ar": sems((1,))},
     )
 
 

time: 36.6 us -> 35.7 us (0.975)
  Pallas kernels: 35.5 us -> 34.7 us
    pallas_call x1, Pallas kernels: 35.5 us -> 34.7 us  [shards(): pl.pallas_call(kernel, out_shape=pltpu.VMEM((ROWS, D), BF16), in_specs=[h...]
where the time goes in v9:
time: 35.7 us; the launch traced here: 35.6 us
  Pallas kernels  34.7 us (97%)
  local copies, waits for them, and re-layouts  0.97 us (3%)
    pallas_call x1, Pallas kernels, shards(): pl.pallas_call(kernel, out_shape=pltpu.VMEM((ROWS, D), BF16), in_specs=[h...  34.7 us
    unnamed x1, local copies, waits for them, and re-layouts  0.97 us

profile of v9, /device:TPU:1, one launch (start us, length us, event | category | flops | bytes accessed | tf_op | source)
XLA Modules:
  0.0 35.6 jit_solution(10126072329339932215)
XLA Ops:
  0.0 34.7 %shard_map.163 = bf16[256,2048]{1,0:T(8,128)(2,1)S(1)} custom-call(bf16[256,2048]{1,0:T(8,128)(2,1)} %latent.1, bf16[32,2048]{1,0:T(8,128)(2,1)} %context.1, bf16[16,128]{1,0:T(8,128)(2,1)} %bitcast.9, bf16[16,128]{1,0:T(8,128)(2,1)} %bitcast.10, bf16[128,256]{1,0:T(8,128)(2,1)} %shift_w.1, bf16[128,256]{1,0:T(8,128)(2,1)} %scale_w.1, ...), custom_call_target="tpu_custom_call" | custom-call | tf_op jit(solution)/shard_map/pallas_call | solution.py:677
  34.7 1.0 %copy.19 = bf16[256,2048]{1,0:T(8,128)(2,1)} copy(bf16[256,2048]{1,0:T(8,128)(2,1)S(1)} %shard_map.163) | data formatting | bytes 2097152
